TPU v7x, 32 devices: a whole 2x2x4 slice. The times are simulated.
32 devices in a mesh: fs: 4 (over z), rep: 4 (over y, x), tp: 2 (over core).
Axes of the slice: x: 2, y: 2, z: 4, core: 2. Of those that a mesh axis runs over, the one named last changes fastest.
Arguments:
- saved_input: bfloat16 [5632, 2048], P(('fs', 'rep')), may hold values from -6 to 6
- query_cot: bfloat16 [5632, 1024], P(('fs', 'rep'), 'tp'), may hold values from -0.078125 to 0.078125
- attn_out: bfloat16 [5632, 1024], P(('fs', 'rep'), 'tp'), may hold values from -6 to 6
- out_cot: bfloat16 [5632, 2048], P(('fs', 'rep')), may hold values from -0.078125 to 0.078125
- query_basis: bfloat16 [2048, 512], P('fs'), may hold values from -0.25 to 0.25
- output_basis: bfloat16 [2048, 512], P('fs'), may hold values from -0.25 to 0.25
- query_weight: float32 [2048, 1024], P('fs', 'tp'), may hold values from -6 to 6
- output_weight: float32 [1024, 2048], P('tp', 'fs'), may hold values from -6 to 6
- query_moment: float32 [512, 1024], P('rep', 'tp'), may hold values from -52 to 52
- output_moment: float32 [1024, 512], P('tp', 'rep'), may hold values from -52 to 52
Outputs:
- query_step: float32 [2048, 1024], P('fs', 'tp')
- output_step: float32 [1024, 2048], P('tp', 'fs')
- query_new: float32 [2048, 1024], P('fs', 'tp')
- output_new: float32 [1024, 2048], P('tp', 'fs')
- query_copy: bfloat16 [2048, 1024], P('fs', 'tp')
- output_copy: bfloat16 [1024, 2048], P('tp', 'fs')
- query_moment_new: float32 [512, 1024], P('rep', 'tp')
- output_moment_new: float32 [1024, 512], P('tp', 'rep')
All inputs are finite; a program needn't handle non-finite values.
Results may differ from a plain program's by a relative error of at most 0.0029.
Values may be sent and summed in bfloat16 or wider, within the bound.
No kernel may reach another device: no remote copies, remote signals or barrier semaphores. Data moves between devices by JAX's collectives and lax.ppermute only.
A program may use at most 64 MiB of HBM per device.

v0:
```python
import jax
import jax.numpy as jnp
from jax import lax
from jax.sharding import PartitionSpec as P

BETA = 0.8
RATE = 0.2
EPS = 1e-06


def on_device(
    saved_input,
    query_cot,
    attn_out,
    out_cot,
    query_basis,
    output_basis,
    query_weight,
    output_weight,
    query_moment,
    output_moment,
):
    rank = query_basis.shape[1]
    grad_rows = lax.psum_scatter(
        jnp.dot(saved_input.T, query_cot, preferred_element_type=jnp.float32),
        "fs",
        scatter_dimension=0,
        tiled=True,
    )
    query_part = jnp.dot(
        query_basis.astype(jnp.float32).T, grad_rows, precision=lax.Precision.HIGHEST
    )
    cot_proj = jnp.dot(
        out_cot,
        lax.all_gather(output_basis, "fs", axis=0, tiled=True),
        preferred_element_type=jnp.float32,
    )
    output_part = jnp.dot(attn_out.astype(jnp.float32).T, cot_proj, precision=lax.Precision.HIGHEST)
    reps = lax.axis_size("rep")
    share = rank // reps
    query_terms, output_terms = (
        lax.all_to_all(
            query_part.astype(jnp.bfloat16), "rep", split_axis=0, concat_axis=0, tiled=True
        ).astype(query_part.dtype),
        lax.all_to_all(
            output_part.T.astype(jnp.bfloat16), "rep", split_axis=0, concat_axis=0, tiled=True
        ).astype(jnp.float32),
    )
    width = query_part.shape[1]
    query_local = jnp.sum(query_terms.reshape(reps, share, width), axis=0)
    output_local = jnp.sum(output_terms.reshape(reps, share, width), axis=0)
    query_share, output_flip = lax.psum((query_local, output_local), "fs")
    output_share = output_flip.T
    query_moment_new = BETA * query_moment + (1.0 - BETA) * query_share
    output_moment_new = BETA * output_moment + (1.0 - BETA) * output_share
    query_squares, output_squares = lax.psum(
        (
            jnp.sum(query_moment_new * query_moment_new),
            jnp.sum(output_moment_new * output_moment_new),
        ),
        ("rep", "tp"),
    )
    entries = rank * query_moment.shape[1] * lax.axis_size("tp")
    query_dir = (query_moment_new * lax.rsqrt(query_squares / entries + EPS)).astype(jnp.bfloat16)
    output_dir = (output_moment_new * lax.rsqrt(output_squares / entries + EPS)).astype(
        jnp.bfloat16
    )
    query_full, output_full = (
        lax.all_gather(query_dir, "rep", axis=0, tiled=True),
        lax.all_gather(output_dir, "rep", axis=1, tiled=True),
    )
    query_step = jnp.dot(query_basis, query_full, preferred_element_type=jnp.float32)
    output_step = jnp.dot(output_full, output_basis.T, preferred_element_type=jnp.float32)
    query_new = query_weight - RATE * query_step
    output_new = output_weight - RATE * output_step
    return (
        query_step,
        output_step,
        query_new,
        output_new,
        query_new.astype(jnp.bfloat16),
        output_new.astype(jnp.bfloat16),
        query_moment_new,
        output_moment_new,
    )


def solution(mesh):
    placed = (
        P(("fs", "rep"), None),
        P(("fs", "rep"), "tp"),
        P(("fs", "rep"), "tp"),
        P(("fs", "rep"), None),
        P("fs", None),
        P("fs", None),
        P("fs", "tp"),
        P("tp", "fs"),
        P("rep", "tp"),
        P("tp", "rep"),
    )
    return jax.shard_map(
        on_device,
        mesh=mesh,
        in_specs=placed,
        out_specs=(
            P("fs", "tp"),
            P("tp", "fs"),
            P("fs", "tp"),
            P("tp", "fs"),
            P("fs", "tp"),
            P("tp", "fs"),
            P("rep", "tp"),
            P("tp", "rep"),
        ),
        check_vma=False,
    )
```

profile of v0, /device:TPU:0, one launch (start us, length us, event | category | flops | bytes accessed | tf_op | source)
XLA Modules:
  0.0 253.2 jit_solution(7196778270909197220)
XLA Ops:
  8.5 4.2 %fusion.2 = f32[2048,512]{1,0:T(8,128)} fusion(bf16[352,2048]{1,0:T(8,128)(2,1)S(1)} %copy-done, bf16[352,512]{1,0:T(8,128)(2,1)} %param.11), kind=kOutput, calls=%fused_computation.15 | convolution fusion | flops 738197504 | bytes 5996544 | tf_op jit(solution)/shard_map/dot_general | solution.py:25
  12.8 45.2 %all-gather.2.cloned.1.call-done = bf16[2048,512]{1,0:T(8,128)(2,1)} async-done(((bf16[512,512]{1,0:T(8,128)(2,1)}), bf16[2048,512]{1,0:T(8,128)(2,1)}) %all-gather.2.cloned.1.call-update) | async-done | bytes 2097168 | tf_op jit(solution)/shard_map/all_gather | solution.py:35
  58.0 2.9 %fusion.3 = f32[352,512]{1,0:T(8,128)S(1)} fusion(bf16[352,2048]{1,0:T(8,128)(2,1)} %param.13, bf16[2048,512]{1,0:T(8,128)(2,1)} %all-gather.2.cloned.1.call-done), kind=kOutput, calls=%fused_computation.16 | convolution fusion | flops 738197504 | bytes 4259840 | tf_op jit(solution)/shard_map/dot_general | solution.py:33
  60.9 1.8 convolution_convert_fusion
  62.8 3.7 %all-to-all-start.1 = ((bf16[4,128,512]{2,1,0:T(8,128)(2,1)}), bf16[4,128,512]{2,1,0:T(8,128)(2,1)S(1)}, u32[]{:S(2)}, u32[]{:S(2)}) async-start(bf16[4,128,512]{2,1,0:T(8,128)(2,1)} %bitcast.3), calls=%async_computation.2 | async-start | bytes 1048576 | tf_op jit(solution)/shard_map/all_to_all | solution.py:45
  66.4 69.5 %reduce-scatter.2.cloned.1.call-done = f32[512,512]{1,0:T(8,128)} async-done(((f32[2048,512]{1,0:T(8,128)}), f32[512,512]{1,0:T(8,128)}) %reduce-scatter.2.cloned.1.call-update) | async-done | bytes 1048592 | tf_op jit(solution)/shard_map/reduce_scatter | solution.py:24
  135.9 3.1 %convolution_convert_fusion.1 = bf16[512,512]{0,1:T(8,128)(2,1)} fusion(f32[512,512]{1,0:T(8,128)} %reduce-scatter.2.cloned.1.call-done, bf16[512,512]{1,0:T(8,128)(2,1)S(1)} %copy-done.4), kind=kOutput, calls=%fused_computation.2 | convolution fusion | flops 1610874880 | bytes 2097152 | tf_op jit(solution)/shard_map/dot_general | solution.py:30
  139.0 3.7 %all-to-all-start = ((bf16[4,128,512]{2,1,0:T(8,128)(2,1)}), bf16[4,128,512]{2,1,0:T(8,128)(2,1)S(1)}, u32[]{:S(2)}, u32[]{:S(2)}) async-start(bf16[4,128,512]{2,1,0:T(8,128)(2,1)} %bitcast.1), calls=%async_computation.1 | async-start | bytes 1048576 | tf_op jit(solution)/shard_map/all_to_all | solution.py:42
  143.4 7.0 %all-to-all-done = bf16[4,128,512]{2,1,0:T(8,128)(2,1)S(1)} async-done(((bf16[4,128,512]{2,1,0:T(8,128)(2,1)}), bf16[4,128,512]{2,1,0:T(8,128)(2,1)S(1)}, u32[]{:S(2)}, u32[]{:S(2)}) %all-to-all-start) | async-done | bytes 524320 | tf_op jit(solution)/shard_map/all_to_all | solution.py:42
  152.4 2.6 %copy.29 = f32[512,512]{0,1:T(8,128)} copy(f32[512,512]{1,0:T(8,128)} %param.16) | data formatting | bytes 2097152 | tf_op args[6]
  155.0 34.8 %all-reduce.4.cloned.1.call-done = (f32[128,512]{1,0:T(8,128)}, f32[128,512]{1,0:T(8,128)}) async-done(((f32[128,512]{1,0:T(8,128)}, f32[128,512]{1,0:T(8,128)}), (f32[128,512]{1,0:T(8,128)}, f32[128,512]{1,0:T(8,128)})) %all-reduce.4.cloned.1.call-update) | async-done | bytes 524304 | tf_op jit(solution)/shard_map/psum | solution.py:52
  189.8 1.6 multiply_reduce_fusion
  191.5 2.3 multiply_reduce_fusion.1
  193.8 13.3 %all-reduce = (f32[]{:T(128)}, f32[]{:T(128)}) all-reduce(f32[]{:T(128)} %get-tuple-element.34, f32[]{:T(128)} %get-tuple-element.32), channel_id=1, replica_groups=mesh['fs'=4,'rep'=4,'tp'=2] {'rep','tp'}, use_global_device_ids=true, to_apply=%region_4.0 | all-reduce | flops 2 | bytes 16 | tf_op jit(solution)/shard_map/psum | solution.py:56
  208.7 9.1 %all_gather.11 = bf16[512,512]{0,1:T(8,128)(2,1)S(1)} all-gather(bf16[512,128]{0,1:T(8,128)(2,1)S(1)} %multiply_convert_fusion), channel_id=1, replica_groups=mesh['fs'=4,'rep'=4,'tp'=2] {'rep'}, dimensions={1}, use_global_device_ids=true | all-gather | bytes 655360 | tf_op jit(solution)/shard_map/all_gather | solution.py:70
  217.8 1.5 fusion.4
  220.3 1.3 copy.30
  221.6 2.3 fusion
  223.8 1.3 copy.34
  225.2 2.1 copy.36
  229.0 10.2 %all_gather.9 = bf16[512,512]{1,0:T(8,128)(2,1)S(1)} all-gather(bf16[128,512]{1,0:T(8,128)(2,1)S(1)} %multiply_convert_fusion.1), channel_id=1, replica_groups=mesh['fs'=4,'rep'=4,'tp'=2] {'rep'}, dimensions={0}, use_global_device_ids=true | all-gather | bytes 655360 | tf_op jit(solution)/shard_map/all_gather | solution.py:69
  239.1 2.7 %fusion.1 = (bf16[512,512]{0,1:T(8,128)(2,1)}, f32[512,512]{0,1:T(8,128)S(1)}, f32[512,512]{0,1:T(8,128)}) fusion(f32[512,512]{0,1:T(8,128)S(1)} %copy-done.2, bf16[512,512]{1,0:T(8,128)(2,1)S(1)} %all_gather.9, bf16[512,512]{1,0:T(8,128)(2,1)} %param.14), kind=kOutput, calls=%fused_computation.14 | convolution fusion | flops 269221888 | bytes 4718592 | tf_op jit(solution)/shard_map/dot_general | solution.py:72
  241.8 2.5 copy.32
  244.4 1.3 copy.33
  (35 shorter events, 7.9 us)
Async XLA Ops:
  7.2 1.4 copy-start
  7.2 50.8 %all-gather.2.cloned.1.call-start = ((), (), s32[]{:S(2)}) async-start(), calls=%async_computation.4 | async-start | bytes 2621440 | tf_op jit(solution)/shard_map/all_gather | solution.py:35
  7.9 128.0 %reduce-scatter.2.cloned.1.call-start = ((), (), s32[]{:S(2)}) async-start(), calls=%async_computation.3 | async-start | bytes 5242880 | tf_op jit(solution)/shard_map/reduce_scatter | solution.py:24
  12.8 48.1 %copy-start.7 = (bf16[352,512]{1,0:T(8,128)(2,1)S(1)}, bf16[352,512]{1,0:T(8,128)(2,1)}, u32[]{:S(2)}) copy-start(bf16[352,512]{1,0:T(8,128)(2,1)} %param.12) | copy-start | bytes 1081348
  60.9 75.0 %copy-start.4 = (bf16[512,512]{1,0:T(8,128)(2,1)S(1)}, bf16[512,512]{1,0:T(8,128)(2,1)}, u32[]{:S(2)}) copy-start(bf16[512,512]{1,0:T(8,128)(2,1)} %param.14) | copy-start | bytes 1572868
  62.8 76.2 %all-to-all-start.1 = ((bf16[4,128,512]{2,1,0:T(8,128)(2,1)}), bf16[4,128,512]{2,1,0:T(8,128)(2,1)S(1)}, u32[]{:S(2)}, u32[]{:S(2)}) async-start(bf16[4,128,512]{2,1,0:T(8,128)(2,1)} %bitcast.3), calls=%async_computation.2 | async-start | bytes 1048576 | tf_op jit(solution)/shard_map/all_to_all | solution.py:45
  139.0 11.4 %all-to-all-start = ((bf16[4,128,512]{2,1,0:T(8,128)(2,1)}), bf16[4,128,512]{2,1,0:T(8,128)(2,1)S(1)}, u32[]{:S(2)}, u32[]{:S(2)}) async-start(bf16[4,128,512]{2,1,0:T(8,128)(2,1)} %bitcast.1), calls=%async_computation.1 | async-start | bytes 1048576 | tf_op jit(solution)/shard_map/all_to_all | solution.py:42
  142.6 9.4 %copy-start.5 = (f32[512,512]{1,0:T(8,128)S(1)}, f32[512,512]{1,0:T(8,128)}, u32[]{:S(2)}) copy-start(f32[512,512]{1,0:T(8,128)} %param.17) | copy-start | bytes 3145732
  142.6 47.2 %all-reduce.4.cloned.1.call-start = ((), (), s32[]{:S(2)}) async-start(), calls=%async_computation.5 | async-start | bytes 1048576 | tf_op jit(solution)/shard_map/psum | solution.py:52
  143.4 7.8 %copy-start.8 = (f32[512,128]{1,0:T(8,128)S(1)}, f32[512,128]{1,0:T(8,128)}, u32[]{:S(2)}) copy-start(f32[512,128]{1,0:T(8,128)} %param.19) | copy-start | bytes 786436
  152.4 37.4 %copy-start.6 = (f32[512,128]{0,1:T(8,128)S(1)}, f32[512,128]{0,1:T(8,128)}, u32[]{:S(2)}) copy-start(f32[512,128]{0,1:T(8,128)} %copy.28) | copy-start | bytes 786436
  152.4 39.1 %copy-start.9 = (f32[128,512]{1,0:T(8,128)S(1)}, f32[128,512]{1,0:T(8,128)}, u32[]{:S(2)}) copy-start(f32[128,512]{1,0:T(8,128)} %param.18) | copy-start | bytes 786436
  219.3 1.0 copy-start.1
  225.2 14.0 %copy-start.2 = (f32[512,512]{0,1:T(8,128)S(1)}, f32[512,512]{0,1:T(8,128)}, u32[]{:S(2)}) copy-start(f32[512,512]{0,1:T(8,128)} %copy.29) | copy-start | bytes 3145732
  244.4 1.3 copy-start.3
Sparse Core Ops, SparseCore 0:
  9.6 48.3 all-gather.1
  60.3 75.5 reduce-scatter.1
  151.3 38.4 all-reduce.3
where the time goes:
time: 254 us; the launch traced here: 253 us
  waiting for transfers between devices  157 us (62%)
  blocking collectives  32.6 us (13%)
  matrix products  16.3 us (6%)
  local copies, waits for them, and re-layouts  15.8 us (6%)
  between operations  15.2 us (6%)
  other arithmetic  8.72 us (3%)
  starting transfers between devices  7.38 us (3%)
    reduce_scatter x1, waiting for transfers between devices, on_device(): lax.psum_scatter(jnp.dot(saved_input.T, query_cot, preferred_element_type...  69.5 us
    all_gather x1, waiting for transfers between devices, on_device(): lax.all_gather(output_basis, 'fs', axis=0, tiled=True)  45.2 us
    psum x1, waiting for transfers between devices, on_device(): query_share, output_flip = lax.psum((query_local, output_local), 'fs')  34.8 us
    unnamed x29, local copies, waits for them, and re-layouts  14.5 us
    psum x1, blocking collectives, on_device(): lax.psum((jnp.sum(query_moment_new * query_moment_new), jnp.sum(output_mo...  13.3 us
    all_gather x1, blocking collectives, on_device(): lax.all_gather(query_dir, 'rep', axis=0, tiled=True)  10.2 us
    all_gather x1, blocking collectives, on_device(): lax.all_gather(output_dir, 'rep', axis=1, tiled=True)  9.09 us
    all_to_all x1, waiting for transfers between devices, on_device(): lax.all_to_all(query_part.astype(jnp.bfloat16), 'rep', split_axis=0, conc...  7.01 us
  transfers between devices with their start and end apart: 5, of which 4 were waited for; matrix products, arithmetic and copies ran while one was open for 7% of the time, Pallas kernels for 0%

commit v1 on v0

--- a/solution.py
+++ b/solution.py
@@ -1,11 +1,266 @@
 import jax
 import jax.numpy as jnp
 from jax import lax
+from jax.experimental import pallas as pl
+from jax.experimental.pallas import tpu as pltpu
 from jax.sharding import PartitionSpec as P
 
 BETA = 0.8
 RATE = 0.2
 EPS = 1e-06
+BF16 = jnp.bfloat16
+F32 = jnp.float32
+SMEM = pl.BlockSpec(memory_space=pltpu.SMEM)
+VMEM = pl.BlockSpec(memory_space=pltpu.VMEM)
+
+
+def shift(x, axis, k):
+    n = lax.axis_size(axis)
+    return lax.ppermute(x, axis, [(i, (i + k) % n) for i in range(n)])
+
+
+def flip(x, axis, m):
+    return lax.ppermute(x, axis, [(i, i ^ m) for i in range(lax.axis_size(axis))])
+
+
+def call(kernel, ids, args, outs, scratch=()):
+    return pl.pallas_call(
+        kernel,
+        out_shape=outs,
+        in_specs=[SMEM] + [VMEM] * len(args),
+        out_specs=jax.tree.map(lambda _: VMEM, outs),
+        scratch_shapes=scratch,
+    )(ids, *args)
+
+
+def project(ids, tokens, basis, own, mates):
+    fs, reps = lax.axis_size("fs"), len(mates) + 1
+    rows, half = basis.shape[0], own.shape[1]
+    chunk = rows // reps
+
+    def kernel(ids, tokens, basis, *rest):
+        groups, out, whole = rest[:reps], rest[reps], rest[reps + 1]
+        f, r, t = ids[0], ids[1], ids[2]
+        whole[pl.ds(pl.multiple_of(f * rows, rows), rows), :] = basis[
+            :, pl.ds(pl.multiple_of(t * half, half), half)
+        ]
+        for m, group in enumerate(groups):
+            for k in range(1, fs):
+                at = lax.rem(f + fs - k, fs) * rows + (r ^ m) * chunk
+                whole[pl.ds(pl.multiple_of(at, chunk), chunk), :] = group[
+                    (k - 1) * chunk : k * chunk, :
+                ]
+        out[...] = jnp.dot(tokens[...], whole[...], preferred_element_type=F32).astype(BF16)
+
+    return call(
+        kernel,
+        ids,
+        [tokens, basis, own, *mates],
+        jax.ShapeDtypeStruct((tokens.shape[0], half), BF16),
+        [pltpu.VMEM((fs * rows, half), BF16)],
+    )
+
+
+def contract(ids, mine, other, local, reps, flat):
+    rows, half = mine.shape
+    rank, width = 2 * half, local.shape[1]
+    share = rank // reps
+    shape = (width, share) if flat else (share, width)
+
+    def kernel(ids, mine, other, local, keep, *rest):
+        sends, both = rest[: reps - 1], rest[reps - 1]
+        r, t = ids[1], ids[2]
+        both[:, pl.ds(pl.multiple_of(t * half, half), half)] = mine[...]
+        both[:, pl.ds(pl.multiple_of((1 - t) * half, half), half)] = other[...]
+        for m in range(reps):
+            part = both[:, pl.ds(pl.multiple_of((r ^ m) * share, share), share)]
+            pair = (local[...], part) if flat else (part, local[...])
+            block = lax.dot_general(*pair, (((0,), (0,)), ((), ())), preferred_element_type=F32)
+            if m:
+                sends[m - 1][...] = block.astype(BF16)
+            else:
+                keep[...] = block
+
+    return call(
+        kernel,
+        ids,
+        [mine, other, local],
+        [jax.ShapeDtypeStruct(shape, F32)] + [jax.ShapeDtypeStruct(shape, BF16)] * (reps - 1),
+        [pltpu.VMEM((rows, rank), BF16)],
+    )
+
+
+def add_and_split(ids, keep, terms):
+    fs = lax.axis_size("fs")
+    rows, width = keep.shape
+    size = rows // fs
+
+    def kernel(ids, keep, *rest):
+        terms, own, sends, total = rest[: len(terms_)], rest[-fs - 1], rest[-fs:-1], rest[-1]
+        f = ids[0]
+        value = keep[...]
+        for term in terms:
+            value = value + term[...].astype(F32)
+        total[...] = value
+        for k in range(fs):
+            at = pl.multiple_of(lax.rem(f + k, fs) * size, size)
+            part = total[pl.ds(at, size), :]
+            if k:
+                sends[k - 1][...] = part.astype(BF16)
+            else:
+                own[...] = part
+
+    terms_ = terms
+    return call(
+        kernel,
+        ids,
+        [keep, *terms],
+        [jax.ShapeDtypeStruct((size, width), F32)]
+        + [jax.ShapeDtypeStruct((size, width), BF16)] * (fs - 1),
+        [pltpu.VMEM((rows, width), F32)],
+    )
+
+
+def advance(ids, moment, pieces):
+    fs = len(pieces)
+    rows, width = moment.shape
+    size = rows // fs
+
+    def kernel(ids, moment, *rest):
+        pieces, (new, rounded, squares) = rest[:fs], rest[fs:]
+        f = ids[0]
+        for k, piece in enumerate(pieces):
+            at = pl.ds(pl.multiple_of(lax.rem(f + fs - k, fs) * size, size), size)
+            new[at, :] = BETA * moment[at, :] + (1.0 - BETA) * piece[...].astype(F32)
+        value = new[...]
+        rounded[...] = value.astype(BF16)
+        value = jnp.sum((value * value).reshape(rows // 8, 8, width), axis=0)
+        lanes = value[:, :128]
+        for j in range(1, width // 128):
+            lanes = lanes + value[:, j * 128 : (j + 1) * 128]
+        squares[...] = lanes
+
+    return call(
+        kernel,
+        ids,
+        [moment, *pieces],
+        [
+            jax.ShapeDtypeStruct((rows, width), F32),
+            jax.ShapeDtypeStruct((rows, width), BF16),
+            jax.ShapeDtypeStruct((8, 128), F32),
+        ],
+    )
+
+
+def finish(ids, squares, entries, basis, blocks, weight, flat):
+    reps = len(blocks)
+    rows, width = weight.shape
+    rank = basis.shape[1]
+    share = rank // reps
+    tile = min(rows, 128)
+    full = (rows, rank) if flat else (rank, width)
+
+    def kernel(ids, squares, basis, *rest):
+        blocks, weight, step, new, copy, whole = rest[:reps], *rest[reps:]
+        r = ids[1]
+
+        @pl.when(pl.program_id(0) == 0)
+        def _():
+            for m, block in enumerate(blocks):
+                at = pl.ds(pl.multiple_of((r ^ m) * share, share), share)
+                if flat:
+                    whole[:, at] = block[...]
+                else:
+                    whole[at, :] = block[...]
+
+        scale = lax.rsqrt(jnp.sum(squares[...]) * (1.0 / entries) + EPS)
+        if flat:
+            i = pl.multiple_of(pl.program_id(0) * tile, tile)
+            value = lax.dot_general(
+                whole[pl.ds(i, tile), :],
+                basis[...],
+                (((1,), (1,)), ((), ())),
+                preferred_element_type=F32,
+            )
+        else:
+            value = jnp.dot(basis[...], whole[...], preferred_element_type=F32)
+        value = value * scale
+        step[...] = value
+        value = weight[...] - RATE * value
+        new[...] = value
+        copy[...] = value.astype(BF16)
+
+    by_rows = pl.BlockSpec((tile, width), lambda i: (i, 0))
+    basis_spec = VMEM if flat else pl.BlockSpec((tile, rank), lambda i: (i, 0))
+    return pl.pallas_call(
+        kernel,
+        grid=(rows // tile,),
+        out_shape=[
+            jax.ShapeDtypeStruct(weight.shape, F32),
+            jax.ShapeDtypeStruct(weight.shape, F32),
+            jax.ShapeDtypeStruct(weight.shape, BF16),
+        ],
+        in_specs=[SMEM, VMEM, basis_spec] + [VMEM] * reps + [by_rows],
+        out_specs=[by_rows] * 3,
+        scratch_shapes=[pltpu.VMEM(full, BF16)],
+    )(ids, squares, basis, *blocks, weight)
+
+
+def stream(ids, tokens, local, basis, weight, moment, flat):
+    fs, reps, tps = (lax.axis_size(axis) for axis in ("fs", "rep", "tp"))
+    rows, rank = basis.shape
+    chunk, half = rows // reps, rank // tps
+    piece = lax.dynamic_slice(basis, (ids[1] * chunk, ids[2] * half), (chunk, half))
+    own = jnp.concatenate([shift(piece, "fs", k) for k in range(1, fs)])
+    mine = project(ids, tokens, basis, own, [flip(own, "rep", m) for m in range(1, reps)])
+    keep, *sends = contract(ids, mine, flip(mine, "tp", 1), local, reps, flat)
+    terms = [flip(send, "rep", m + 1) for m, send in enumerate(sends)]
+    part, *sends = add_and_split(ids, keep, terms)
+    for k, send in enumerate(sends):
+        part = part + shift(send, "fs", k + 1).astype(F32)
+    part = part.astype(BF16)
+    new, rounded, squares = advance(
+        ids, moment, [part] + [shift(part, "fs", k) for k in range(1, fs)]
+    )
+    blocks = [rounded] + [flip(rounded, "rep", m) for m in range(1, reps)]
+    squares = squares + flip(squares, "tp", 1)
+    bit = 1
+    while bit < reps:
+        squares = squares + flip(squares, "rep", bit)
+        bit *= 2
+    entries = moment.size * reps * tps
+    return *finish(ids, squares, entries, basis, blocks, weight, flat), new
+
+
+def direct(
+    saved_input,
+    query_cot,
+    attn_out,
+    out_cot,
+    query_basis,
+    output_basis,
+    query_weight,
+    output_weight,
+    query_moment,
+    output_moment,
+):
+    ids = jnp.stack([lax.axis_index(axis) for axis in ("fs", "rep", "tp")]).astype(jnp.int32)
+    query_step, query_new, query_copy, query_moment_new = stream(
+        ids, saved_input, query_cot, query_basis, query_weight, query_moment, False
+    )
+    output_step, output_new, output_copy, output_moment_new = stream(
+        ids, out_cot, attn_out, output_basis, output_weight, output_moment, True
+    )
+    return (
+        query_step,
+        output_step,
+        query_new,
+        output_new,
+        query_copy,
+        output_copy,
+        query_moment_new,
+        output_moment_new,
+    )
 
 
 def on_device(
@@ -98,8 +353,9 @@
         P("rep", "tp"),
         P("tp", "rep"),
     )
+    small = mesh.shape["fs"] <= 4 and mesh.shape["rep"] == 4 and mesh.shape["tp"] == 2
     return jax.shard_map(
-        on_device,
+        direct if small else on_device,
         mesh=mesh,
         in_specs=placed,
         out_specs=(

time: 254 us -> 125 us (0.49)
  waiting for transfers between devices: 157 us -> 24.8 us
  starting transfers between devices: 7.38 us -> 54.5 us
  blocking collectives: 32.6 us -> 0 us
  Pallas kernels: 0 us -> 27.2 us
  matrix products: 16.3 us -> 0 us
  between operations: 15.2 us -> 0.9 us
  local copies, waits for them, and re-layouts: 15.8 us -> 11.5 us
  other arithmetic: 8.72 us -> 4.93 us
    reduce_scatter x1 -> x0, waiting for transfers between devices: 69.5 us -> none  [on_device(): lax.psum_scatter(jnp.dot(saved_input.T, query_cot, preferred_element_type...]
    ppermute x0 -> x44, starting transfers between devices: none -> 54.5 us  [the longest x18 27.3 us: shift(): return lax.ppermute(x, axis, [(i, (i + k) % n) for i in range(n)])]
    all_gather x1 -> x0, waiting for transfers between devices: 45.2 us -> none  [on_device(): lax.all_gather(output_basis, 'fs', axis=0, tiled=True)]
    psum x1 -> x0, waiting for transfers between devices: 34.8 us -> none  [on_device(): query_share, output_flip = lax.psum((query_local, output_local), 'fs')]
    pallas_call x0 -> x10, Pallas kernels: none -> 27.2 us  [the longest x8 18 us: call(): pl.pallas_call(kernel, out_shape=outs, in_specs=[SMEM] + [VMEM] * len(arg...]
    ppermute x0 -> x44, waiting for transfers between devices: none -> 24.8 us  [the longest x26 17.4 us: flip(): lax.ppermute(x, axis, [(i, i ^ m) for i in range(lax.axis_size(axis))])]
    all_gather x2 -> x0, blocking collectives: 19.3 us -> none  [the longest x1 10.2 us: on_device(): lax.all_gather(query_dir, 'rep', axis=0, tiled=True)]
    dot_general x6 -> x0, matrix products: 16.3 us -> none  [the longest x1 4.22 us: on_device(): jnp.dot(saved_input.T, query_cot, preferred_element_type=jnp.float32)]
  transfers between devices with their start and end apart: 5 -> 44, of which waited for: 4 -> 17; matrix products, arithmetic and copies ran while one was open for 7% -> 5% of each run, Pallas kernels for 0% -> 18%
where the time goes in v1:
time: 125 us; the launch traced here: 124 us
  starting transfers between devices  54.5 us (44%)
  Pallas kernels  27.2 us (22%)
  waiting for transfers between devices  24.8 us (20%)
  local copies, waits for them, and re-layouts  11.5 us (9%)
  other arithmetic  4.93 us (4%)
    ppermute x18, starting transfers between devices, shift(): return lax.ppermute(x, axis, [(i, (i + k) % n) for i in range(n)])  27.3 us
    ppermute x26, starting transfers between devices, flip(): lax.ppermute(x, axis, [(i, i ^ m) for i in range(lax.axis_size(axis))])  27.3 us
    pallas_call x8, Pallas kernels, call(): pl.pallas_call(kernel, out_shape=outs, in_specs=[SMEM] + [VMEM] * len(arg...  18 us
    ppermute x26, waiting for transfers between devices, flip(): lax.ppermute(x, axis, [(i, i ^ m) for i in range(lax.axis_size(axis))])  17.4 us
    unnamed x64, local copies, waits for them, and re-layouts  9.81 us
    pallas_call x2, Pallas kernels, finish(): pl.pallas_call(kernel, grid=(rows // tile,), out_shape=[jax.ShapeDtypeStr...  9.11 us
    ppermute x18, waiting for transfers between devices, shift(): return lax.ppermute(x, axis, [(i, (i + k) % n) for i in range(n)])  7.46 us
  transfers between devices with their start and end apart: 44, of which 17 were waited for; matrix products, arithmetic and copies ran while one was open for 5% of the time, Pallas kernels for 18%

profile of v1, /device:TPU:0, one launch (start us, length us, event | category | flops | bytes accessed | tf_op | source)
XLA Modules:
  0.0 123.9 jit_solution(18259163886665859642)
XLA Ops:
  1.5 3.1 %collective-permute-start.22 = (bf16[128,256]{1,0:T(8,128)(2,1)S(1)}, bf16[128,256]{1,0:T(8,128)(2,1)S(1)}, u32[]{:S(2)}, u32[]{:S(2)}) collective-permute-start(bf16[128,256]{1,0:T(8,128)(2,1)S(1)} %dynamic_slice.7), channel_id=1, source_target_pairs={{0,8},{8,16},{16,24},{24,0},{1,9},{9,17},{17,25},{25,1},{2,10},{10... | collective-permute-start | bytes 196616 | tf_op jit(solution)/shard_map/ppermute | solution.py:19
  4.5 2.0 %collective-permute-start.24 = (bf16[128,256]{1,0:T(8,128)(2,1)S(1)}, bf16[128,256]{1,0:T(8,128)(2,1)S(1)}, u32[]{:S(2)}, u32[]{:S(2)}) collective-permute-start(bf16[128,256]{1,0:T(8,128)(2,1)S(1)} %dynamic_slice.7), channel_id=1, source_target_pairs={{0,24},{8,0},{16,8},{24,16},{1,25},{9,1},{17,9},{25,17},{2,26},{10... | collective-permute-start | bytes 196616 | tf_op jit(solution)/shard_map/ppermute | solution.py:19
  14.1 2.5 %collective-permute-start.27 = (bf16[384,256]{1,0:T(8,128)(2,1)S(1)}, bf16[384,256]{1,0:T(8,128)(2,1)S(1)}, u32[]{:S(2)}, u32[]{:S(2)}) collective-permute-start(bf16[384,256]{1,0:T(8,128)(2,1)S(1)} %constant_dynamic-update-slice_fusion.3.rest_0_), channel_id=1, source_target_pairs={{0,6},{2,4},{4,2},{6,0},{1,7},{3,5},{5,3},{7,1},{8,14},{10,12},{12... | collective-permute-start | bytes 589832 | tf_op jit(solution)/shard_map/ppermute | solution.py:23
  19.2 1.9 %collective-permute-start.5 = (bf16[384,256]{1,0:T(8,128)(2,1)S(1)}, bf16[384,256]{1,0:T(8,128)(2,1)S(1)}, u32[]{:S(2)}, u32[]{:S(2)}) collective-permute-start(bf16[384,256]{1,0:T(8,128)(2,1)S(1)} %constant_dynamic-update-slice_fusion.rest_0_), channel_id=1, source_target_pairs={{0,6},{2,4},{4,2},{6,0},{1,7},{3,5},{5,3},{7,1},{8,14},{10,12},{12... | collective-permute-start | bytes 589832 | tf_op jit(solution)/shard_map/ppermute | solution.py:23
  24.4 4.1 %collective-permute-done.26.rest_2_ = bf16[384,256]{1,0:T(8,128)(2,1)S(1)} collective-permute-done((bf16[384,256]{1,0:T(8,128)(2,1)S(1)}, bf16[384,256]{1,0:T(8,128)(2,1)S(1)}, u32[]{:S(2)}, u32[]{:S(2)}) %collective-permute-start.26) | collective-permute-done | bytes 196640 | tf_op jit(solution)/shard_map/ppermute | solution.py:23
  29.9 3.0 %shard_map.166.mine = bf16[352,256]{1,0:T(8,128)(2,1)} custom-call(s32[3]{0:T(128)} %pad_add_fusion.ids, bf16[352,2048]{1,0:T(8,128)(2,1)} %tokens.3, bf16[512,512]{1,0:T(8,128)(2,1)} %basis.7, bf16[384,256]{1,0:T(8,128)(2,1)} %copy-done, bf16[384,256]{1,0:T(8,128)(2,1)} %copy-done.4, bf16[384,256]{1,0:T(8,128)(2,1)} %copy-done.3, bf16[384,256]{1,0:T(8,128)(2,1)} %copy-done.2), custom_call_target="tpu_custom_call" | custom-call | tf_op jit(solution)/shard_map/pallas_call | solution.py:27
  34.3 3.0 %shard_map.161.mine = bf16[352,256]{1,0:T(8,128)(2,1)} custom-call(s32[3]{0:T(128)} %pad_add_fusion.ids, bf16[352,2048]{1,0:T(8,128)(2,1)} %tokens.2, bf16[512,512]{1,0:T(8,128)(2,1)} %basis.5, bf16[384,256]{1,0:T(8,128)(2,1)} %copy-done.1, bf16[384,256]{1,0:T(8,128)(2,1)} %copy-done.7, bf16[384,256]{1,0:T(8,128)(2,1)} %copy-done.6, bf16[384,256]{1,0:T(8,128)(2,1)} %copy-done.5), custom_call_target="tpu_custom_call" | custom-call | tf_op jit(solution)/shard_map/pallas_call | solution.py:27
  38.5 2.5 %shard_map.167 = (f32[512,128]{1,0:T(8,128)}, bf16[512,128]{1,0:T(8,128)(2,1)}, bf16[512,128]{1,0:T(8,128)(2,1)}, bf16[512,128]{1,0:T(8,128)(2,1)}) custom-call(s32[3]{0:T(128)} %pad_add_fusion.ids, bf16[352,256]{1,0:T(8,128)(2,1)} %shard_map.166.mine, bf16[352,256]{1,0:T(8,128)(2,1)} %copy-done.9, bf16[352,512]{1,0:T(8,128)(2,1)} %local.3), custom_call_target="tpu_custom_call" | custom-call | tf_op jit(solution)/shard_map/pallas_call | solution.py:27
  44.4 2.6 %collective-permute-done.29.rest_0_ = bf16[512,128]{1,0:T(8,128)(2,1)S(1)} collective-permute-done((bf16[512,128]{1,0:T(8,128)(2,1)}, bf16[512,128]{1,0:T(8,128)(2,1)S(1)}, u32[]{:S(2)}, u32[]{:S(2)}) %collective-permute-start.29) | collective-permute-done | bytes 131104 | tf_op jit(solution)/shard_map/ppermute | solution.py:23
  47.0 3.6 %collective-permute-done.30.rest_1_ = bf16[512,128]{1,0:T(8,128)(2,1)S(1)} collective-permute-done((bf16[512,128]{1,0:T(8,128)(2,1)}, bf16[512,128]{1,0:T(8,128)(2,1)S(1)}, u32[]{:S(2)}, u32[]{:S(2)}) %collective-permute-start.30) | collective-permute-done | bytes 131104 | tf_op jit(solution)/shard_map/ppermute | solution.py:23
  51.3 1.8 %shard_map.168 = (f32[128,128]{1,0:T(8,128)}, bf16[128,128]{1,0:T(8,128)(2,1)}, bf16[128,128]{1,0:T(8,128)(2,1)}, bf16[128,128]{1,0:T(8,128)(2,1)}) custom-call(s32[3]{0:T(128)} %pad_add_fusion.ids, f32[512,128]{1,0:T(8,128)} %get-tuple-element.47.keep, bf16[512,128]{1,0:T(8,128)(2,1)} %copy-done.21, bf16[512,128]{1,0:T(8,128)(2,1)} %copy-done.22, ...), custom_call_target="tpu_custom_call" | custom-call | tf_op jit(solution)/shard_map/pallas_call | solution.py:27
  54.8 4.2 %collective-permute-start.33 = (bf16[128,128]{1,0:T(8,128)(2,1)}, bf16[128,128]{1,0:T(8,128)(2,1)S(1)}, u32[]{:S(2)}, u32[]{:S(2)}) collective-permute-start(bf16[128,128]{1,0:T(8,128)(2,1)} %get-tuple-element.53), channel_id=1, source_target_pairs={{0,16},{8,24},{16,0},{24,8},{1,17},{9,25},{17,1},{25,9},{2,18},{10... | collective-permute-start | bytes 98312 | tf_op jit(solution)/shard_map/ppermute | solution.py:19
  59.7 2.3 %shard_map.162 = (f32[128,512]{1,0:T(8,128)}, bf16[128,512]{1,0:T(8,128)(2,1)}, bf16[128,512]{1,0:T(8,128)(2,1)}, bf16[128,512]{1,0:T(8,128)(2,1)}) custom-call(s32[3]{0:T(128)} %pad_add_fusion.ids, bf16[352,256]{1,0:T(8,128)(2,1)} %shard_map.161.mine, bf16[352,256]{1,0:T(8,128)(2,1)} %copy-done.8, bf16[352,512]{1,0:T(8,128)(2,1)} %local.2), custom_call_target="tpu_custom_call" | custom-call | tf_op jit(solution)/shard_map/pallas_call | solution.py:27
  68.1 2.2 %collective-permute-done.8.rest_1_ = bf16[128,512]{1,0:T(8,128)(2,1)S(1)} collective-permute-done((bf16[128,512]{1,0:T(8,128)(2,1)}, bf16[128,512]{1,0:T(8,128)(2,1)S(1)}, u32[]{:S(2)}, u32[]{:S(2)}) %collective-permute-start.8) | collective-permute-done | bytes 131104 | tf_op jit(solution)/shard_map/ppermute | solution.py:23
  71.0 1.9 %shard_map.163 = (f32[32,512]{1,0:T(8,128)}, bf16[32,512]{1,0:T(8,128)(2,1)}, bf16[32,512]{1,0:T(8,128)(2,1)}, bf16[32,512]{1,0:T(8,128)(2,1)}) custom-call(s32[3]{0:T(128)} %pad_add_fusion.ids, f32[128,512]{1,0:T(8,128)} %get-tuple-element.36.keep, bf16[128,512]{1,0:T(8,128)(2,1)} %copy-done.18, bf16[128,512]{1,0:T(8,128)(2,1)} %copy-done.19, ...), custom_call_target="tpu_custom_call" | custom-call | tf_op jit(solution)/shard_map/pallas_call | solution.py:27
  76.4 2.4 %collective-permute-start.11 = (bf16[32,512]{1,0:T(8,128)(2,1)}, bf16[32,512]{1,0:T(8,128)(2,1)S(1)}, u32[]{:S(2)}, u32[]{:S(2)}) collective-permute-start(bf16[32,512]{1,0:T(8,128)(2,1)} %get-tuple-element.42), channel_id=1, source_target_pairs={{0,16},{8,24},{16,0},{24,8},{1,17},{9,25},{17,1},{25,9},{2,18},{10... | collective-permute-start | bytes 98312 | tf_op jit(solution)/shard_map/ppermute | solution.py:19
  78.8 1.7 %collective-permute-start.12 = (bf16[32,512]{1,0:T(8,128)(2,1)}, bf16[32,512]{1,0:T(8,128)(2,1)S(1)}, u32[]{:S(2)}, u32[]{:S(2)}) collective-permute-start(bf16[32,512]{1,0:T(8,128)(2,1)} %get-tuple-element.43), channel_id=1, source_target_pairs={{0,24},{8,0},{16,8},{24,16},{1,25},{9,1},{17,9},{25,17},{2,26},{10... | collective-permute-start | bytes 98312 | tf_op jit(solution)/shard_map/ppermute | solution.py:19
  81.8 1.8 %shard_map.169 = (f32[512,128]{1,0:T(8,128)}, bf16[512,128]{1,0:T(8,128)(2,1)}, f32[8,128]{1,0:T(8,128)}) custom-call(s32[3]{0:T(128)} %pad_add_fusion.ids, f32[512,128]{1,0:T(8,128)} %moment.3, bf16[128,128]{1,0:T(8,128)(2,1)} %copy-done.16, bf16[128,128]{1,0:T(8,128)(2,1)} %copy-done.26, bf16[128,128]{1,0:T(8,128)(2,1)} %copy-done.25, ...), custom_call_target="tpu_custom_call" | custom-call | tf_op jit(solution)/shard_map/pallas_call | solution.py:27
  83.6 1.7 %collective-permute-start.43 = (bf16[512,128]{1,0:T(8,128)(2,1)}, bf16[512,128]{1,0:T(8,128)(2,1)S(1)}, u32[]{:S(2)}, u32[]{:S(2)}) collective-permute-start(bf16[512,128]{1,0:T(8,128)(2,1)} %get-tuple-element.56.rest_0_), channel_id=1, source_target_pairs={{0,6},{2,4},{4,2},{6,0},{1,7},{3,5},{5,3},{7,1},{8,14},{10,12},{12... | collective-permute-start | bytes 393224 | tf_op jit(solution)/shard_map/ppermute | solution.py:23
  88.4 1.7 %collective-permute-done.15.rest_3_ = bf16[32,512]{1,0:T(8,128)(2,1)S(1)} collective-permute-done((bf16[32,512]{1,0:T(8,128)(2,1)S(1)}, bf16[32,512]{1,0:T(8,128)(2,1)S(1)}, u32[]{:S(2)}, u32[]{:S(2)}) %collective-permute-start.15) | collective-permute-done | bytes 32800 | tf_op jit(solution)/shard_map/ppermute | solution.py:19
  90.2 2.1 %collective-permute-done.14.rest_2_ = bf16[32,512]{1,0:T(8,128)(2,1)S(1)} collective-permute-done((bf16[32,512]{1,0:T(8,128)(2,1)S(1)}, bf16[32,512]{1,0:T(8,128)(2,1)S(1)}, u32[]{:S(2)}, u32[]{:S(2)}) %collective-permute-start.14) | collective-permute-done | bytes 32800 | tf_op jit(solution)/shard_map/ppermute | solution.py:19
  94.3 1.8 %shard_map.164 = (f32[128,512]{1,0:T(8,128)}, bf16[128,512]{1,0:T(8,128)(2,1)}, f32[8,128]{1,0:T(8,128)}) custom-call(s32[3]{0:T(128)} %pad_add_fusion.ids, f32[128,512]{1,0:T(8,128)} %moment.2, bf16[32,512]{1,0:T(8,128)(2,1)} %copy-done.17, bf16[32,512]{1,0:T(8,128)(2,1)} %copy-done.29, bf16[32,512]{1,0:T(8,128)(2,1)} %copy-done.28, bf16[32,512]{1,0:T(8,128)(2,1)} %copy-done.27), custom_call_target="tpu_custom_call" | custom-call | tf_op jit(solution)/shard_map/pallas_call | solution.py:27
  113.4 4.7 %shard_map.170 = (f32[512,512]{1,0:T(8,128)}, f32[512,512]{1,0:T(8,128)}, bf16[512,512]{1,0:T(8,128)(2,1)}) custom-call(s32[3]{0:T(128)} %pad_add_fusion.ids, f32[8,128]{1,0:T(8,128)} %add.57.squares, bf16[512,512]{1,0:T(8,128)(2,1)} %basis.7, bf16[512,128]{1,0:T(8,128)(2,1)} %get-tuple-element.56.rest_0_, bf16[512,128]{1,0:T(8,128)(2,1)} %copy-done.14, ...), custom_call_target="tpu_custom_call" | custom-call | tf_op jit(solution)/shard_map/pallas_call | solution.py:195
  119.4 4.5 %shard_map.165 = (f32[512,512]{1,0:T(8,128)}, f32[512,512]{1,0:T(8,128)}, bf16[512,512]{1,0:T(8,128)(2,1)}) custom-call(s32[3]{0:T(128)} %pad_add_fusion.ids, f32[8,128]{1,0:T(8,128)} %add.51.squares, bf16[512,512]{1,0:T(8,128)(2,1)} %basis.5, bf16[128,512]{1,0:T(8,128)(2,1)} %get-tuple-element.45.rest_0_, bf16[128,512]{1,0:T(8,128)(2,1)} %copy-done.15, ...), custom_call_target="tpu_custom_call" | custom-call | tf_op jit(solution)/shard_map/pallas_call | solution.py:195
  (151 shorter events, 59.9 us)
Async XLA Ops:
  1.5 10.0 %collective-permute-start.22 = (bf16[128,256]{1,0:T(8,128)(2,1)S(1)}, bf16[128,256]{1,0:T(8,128)(2,1)S(1)}, u32[]{:S(2)}, u32[]{:S(2)}) collective-permute-start(bf16[128,256]{1,0:T(8,128)(2,1)S(1)} %dynamic_slice.7), channel_id=1, source_target_pairs={{0,8},{8,16},{16,24},{24,0},{1,9},{9,17},{17,25},{25,1},{2,10},{10... | collective-permute-start | bytes 196616 | tf_op jit(solution)/shard_map/ppermute | solution.py:19
  4.5 9.5 %collective-permute-start.24 = (bf16[128,256]{1,0:T(8,128)(2,1)S(1)}, bf16[128,256]{1,0:T(8,128)(2,1)S(1)}, u32[]{:S(2)}, u32[]{:S(2)}) collective-permute-start(bf16[128,256]{1,0:T(8,128)(2,1)S(1)} %dynamic_slice.7), channel_id=1, source_target_pairs={{0,24},{8,0},{16,8},{24,16},{1,25},{9,1},{17,9},{25,17},{2,26},{10... | collective-permute-start | bytes 196616 | tf_op jit(solution)/shard_map/ppermute | solution.py:19
  8.4 10.7 %collective-permute-start.2 = (bf16[128,256]{1,0:T(8,128)(2,1)S(1)}, bf16[128,256]{1,0:T(8,128)(2,1)S(1)}, u32[]{:S(2)}, u32[]{:S(2)}) collective-permute-start(bf16[128,256]{1,0:T(8,128)(2,1)S(1)} %dynamic_slice.6), channel_id=1, source_target_pairs={{0,24},{8,0},{16,8},{24,16},{1,25},{9,1},{17,9},{25,17},{2,26},{10... | collective-permute-start | bytes 196616 | tf_op jit(solution)/shard_map/ppermute | solution.py:19
  9.8 9.4 %collective-permute-start.1 = (bf16[128,256]{1,0:T(8,128)(2,1)S(1)}, bf16[128,256]{1,0:T(8,128)(2,1)S(1)}, u32[]{:S(2)}, u32[]{:S(2)}) collective-permute-start(bf16[128,256]{1,0:T(8,128)(2,1)S(1)} %dynamic_slice.6), channel_id=1, source_target_pairs={{0,16},{8,24},{16,0},{24,8},{1,17},{9,25},{17,1},{25,9},{2,18},{10... | collective-permute-start | bytes 196616 | tf_op jit(solution)/shard_map/ppermute | solution.py:19
  14.1 8.2 %collective-permute-start.27 = (bf16[384,256]{1,0:T(8,128)(2,1)S(1)}, bf16[384,256]{1,0:T(8,128)(2,1)S(1)}, u32[]{:S(2)}, u32[]{:S(2)}) collective-permute-start(bf16[384,256]{1,0:T(8,128)(2,1)S(1)} %constant_dynamic-update-slice_fusion.3.rest_0_), channel_id=1, source_target_pairs={{0,6},{2,4},{4,2},{6,0},{1,7},{3,5},{5,3},{7,1},{8,14},{10,12},{12... | collective-permute-start | bytes 589832 | tf_op jit(solution)/shard_map/ppermute | solution.py:23
  16.6 11.9 %collective-permute-start.26 = (bf16[384,256]{1,0:T(8,128)(2,1)S(1)}, bf16[384,256]{1,0:T(8,128)(2,1)S(1)}, u32[]{:S(2)}, u32[]{:S(2)}) collective-permute-start(bf16[384,256]{1,0:T(8,128)(2,1)S(1)} %constant_dynamic-update-slice_fusion.3.rest_0_), channel_id=1, source_target_pairs={{0,4},{2,6},{4,0},{6,2},{1,5},{3,7},{5,1},{7,3},{8,12},{10,14},{12... | collective-permute-start | bytes 589832 | tf_op jit(solution)/shard_map/ppermute | solution.py:23
  17.6 10.9 %collective-permute-start.25 = (bf16[384,256]{1,0:T(8,128)(2,1)S(1)}, bf16[384,256]{1,0:T(8,128)(2,1)S(1)}, u32[]{:S(2)}, u32[]{:S(2)}) collective-permute-start(bf16[384,256]{1,0:T(8,128)(2,1)S(1)} %constant_dynamic-update-slice_fusion.3.rest_0_), channel_id=1, source_target_pairs={{0,2},{2,0},{4,6},{6,4},{1,3},{3,1},{5,7},{7,5},{8,10},{10,8},{12,... | collective-permute-start | bytes 589832 | tf_op jit(solution)/shard_map/ppermute | solution.py:23
  19.2 13.7 %collective-permute-start.5 = (bf16[384,256]{1,0:T(8,128)(2,1)S(1)}, bf16[384,256]{1,0:T(8,128)(2,1)S(1)}, u32[]{:S(2)}, u32[]{:S(2)}) collective-permute-start(bf16[384,256]{1,0:T(8,128)(2,1)S(1)} %constant_dynamic-update-slice_fusion.rest_0_), channel_id=1, source_target_pairs={{0,6},{2,4},{4,2},{6,0},{1,7},{3,5},{5,3},{7,1},{8,14},{10,12},{12... | collective-permute-start | bytes 589832 | tf_op jit(solution)/shard_map/ppermute | solution.py:23
  21.0 12.0 %collective-permute-start.4 = (bf16[384,256]{1,0:T(8,128)(2,1)S(1)}, bf16[384,256]{1,0:T(8,128)(2,1)S(1)}, u32[]{:S(2)}, u32[]{:S(2)}) collective-permute-start(bf16[384,256]{1,0:T(8,128)(2,1)S(1)} %constant_dynamic-update-slice_fusion.rest_0_), channel_id=1, source_target_pairs={{0,4},{2,6},{4,0},{6,2},{1,5},{3,7},{5,1},{7,3},{8,12},{10,14},{12... | collective-permute-start | bytes 589832 | tf_op jit(solution)/shard_map/ppermute | solution.py:23
  22.3 10.8 %collective-permute-start.3 = (bf16[384,256]{1,0:T(8,128)(2,1)S(1)}, bf16[384,256]{1,0:T(8,128)(2,1)S(1)}, u32[]{:S(2)}, u32[]{:S(2)}) collective-permute-start(bf16[384,256]{1,0:T(8,128)(2,1)S(1)} %constant_dynamic-update-slice_fusion.rest_0_), channel_id=1, source_target_pairs={{0,2},{2,0},{4,6},{6,4},{1,3},{3,1},{5,7},{7,5},{8,10},{10,8},{12,... | collective-permute-start | bytes 589832 | tf_op jit(solution)/shard_map/ppermute | solution.py:23
  37.3 21.7 %collective-permute-start.6 = (bf16[352,256]{1,0:T(8,128)(2,1)}, bf16[352,256]{1,0:T(8,128)(2,1)S(1)}, u32[]{:S(2)}, u32[]{:S(2)}) collective-permute-start(bf16[352,256]{1,0:T(8,128)(2,1)} %shard_map.161.mine), channel_id=1, source_target_pairs={{0,1},{1,0},{2,3},{3,2},{4,5},{5,4},{6,7},{7,6},{8,9},{9,8},{10,11... | collective-permute-start | bytes 540680 | tf_op jit(solution)/shard_map/ppermute | solution.py:23
  42.0 8.6 %collective-permute-start.30 = (bf16[512,128]{1,0:T(8,128)(2,1)}, bf16[512,128]{1,0:T(8,128)(2,1)S(1)}, u32[]{:S(2)}, u32[]{:S(2)}) collective-permute-start(bf16[512,128]{1,0:T(8,128)(2,1)} %get-tuple-element.49), channel_id=1, source_target_pairs={{0,4},{2,6},{4,0},{6,2},{1,5},{3,7},{5,1},{7,3},{8,12},{10,14},{12... | collective-permute-start | bytes 393224 | tf_op jit(solution)/shard_map/ppermute | solution.py:23
  42.8 7.8 %collective-permute-start.31 = (bf16[512,128]{1,0:T(8,128)(2,1)}, bf16[512,128]{1,0:T(8,128)(2,1)S(1)}, u32[]{:S(2)}, u32[]{:S(2)}) collective-permute-start(bf16[512,128]{1,0:T(8,128)(2,1)} %get-tuple-element.50), channel_id=1, source_target_pairs={{0,6},{2,4},{4,2},{6,0},{1,7},{3,5},{5,3},{7,1},{8,14},{10,12},{12... | collective-permute-start | bytes 393224 | tf_op jit(solution)/shard_map/ppermute | solution.py:23
  53.2 10.9 %collective-permute-start.32 = (bf16[128,128]{1,0:T(8,128)(2,1)}, bf16[128,128]{1,0:T(8,128)(2,1)S(1)}, u32[]{:S(2)}, u32[]{:S(2)}) collective-permute-start(bf16[128,128]{1,0:T(8,128)(2,1)} %get-tuple-element.52), channel_id=1, source_target_pairs={{0,8},{8,16},{16,24},{24,0},{1,9},{9,17},{17,25},{25,1},{2,10},{10... | collective-permute-start | bytes 98312 | tf_op jit(solution)/shard_map/ppermute | solution.py:19
  54.8 10.7 %collective-permute-start.33 = (bf16[128,128]{1,0:T(8,128)(2,1)}, bf16[128,128]{1,0:T(8,128)(2,1)S(1)}, u32[]{:S(2)}, u32[]{:S(2)}) collective-permute-start(bf16[128,128]{1,0:T(8,128)(2,1)} %get-tuple-element.53), channel_id=1, source_target_pairs={{0,16},{8,24},{16,0},{24,8},{1,17},{9,25},{17,1},{25,9},{2,18},{10... | collective-permute-start | bytes 98312 | tf_op jit(solution)/shard_map/ppermute | solution.py:19
  62.5 7.8 %collective-permute-start.8 = (bf16[128,512]{1,0:T(8,128)(2,1)}, bf16[128,512]{1,0:T(8,128)(2,1)S(1)}, u32[]{:S(2)}, u32[]{:S(2)}) collective-permute-start(bf16[128,512]{1,0:T(8,128)(2,1)} %get-tuple-element.38), channel_id=1, source_target_pairs={{0,4},{2,6},{4,0},{6,2},{1,5},{3,7},{5,1},{7,3},{8,12},{10,14},{12... | collective-permute-start | bytes 393224 | tf_op jit(solution)/shard_map/ppermute | solution.py:23
  66.4 12.4 %collective-permute-start.37 = (bf16[128,128]{1,0:T(8,128)(2,1)S(1)}, bf16[128,128]{1,0:T(8,128)(2,1)S(1)}, u32[]{:S(2)}, u32[]{:S(2)}) collective-permute-start(bf16[128,128]{1,0:T(8,128)(2,1)S(1)} %add_convert_fusion.rest_0_), channel_id=1, source_target_pairs={{0,24},{8,0},{16,8},{24,16},{1,25},{9,1},{17,9},{25,17},{2,26},{10... | collective-permute-start | bytes 98312 | tf_op jit(solution)/shard_map/ppermute | solution.py:19
  74.9 10.4 %collective-permute-start.10 = (bf16[32,512]{1,0:T(8,128)(2,1)}, bf16[32,512]{1,0:T(8,128)(2,1)S(1)}, u32[]{:S(2)}, u32[]{:S(2)}) collective-permute-start(bf16[32,512]{1,0:T(8,128)(2,1)} %get-tuple-element.41), channel_id=1, source_target_pairs={{0,8},{8,16},{16,24},{24,0},{1,9},{9,17},{17,25},{25,1},{2,10},{10... | collective-permute-start | bytes 98312 | tf_op jit(solution)/shard_map/ppermute | solution.py:19
  76.4 9.0 %collective-permute-start.11 = (bf16[32,512]{1,0:T(8,128)(2,1)}, bf16[32,512]{1,0:T(8,128)(2,1)S(1)}, u32[]{:S(2)}, u32[]{:S(2)}) collective-permute-start(bf16[32,512]{1,0:T(8,128)(2,1)} %get-tuple-element.42), channel_id=1, source_target_pairs={{0,16},{8,24},{16,0},{24,8},{1,17},{9,25},{17,1},{25,9},{2,18},{10... | collective-permute-start | bytes 98312 | tf_op jit(solution)/shard_map/ppermute | solution.py:19
  83.6 25.1 %collective-permute-start.43 = (bf16[512,128]{1,0:T(8,128)(2,1)}, bf16[512,128]{1,0:T(8,128)(2,1)S(1)}, u32[]{:S(2)}, u32[]{:S(2)}) collective-permute-start(bf16[512,128]{1,0:T(8,128)(2,1)} %get-tuple-element.56.rest_0_), channel_id=1, source_target_pairs={{0,6},{2,4},{4,2},{6,0},{1,7},{3,5},{5,3},{7,1},{8,14},{10,12},{12... | collective-permute-start | bytes 393224 | tf_op jit(solution)/shard_map/ppermute | solution.py:23
  104.2 7.8 %collective-permute-start.42 = (bf16[512,128]{1,0:T(8,128)(2,1)}, bf16[512,128]{1,0:T(8,128)(2,1)S(1)}, u32[]{:S(2)}, u32[]{:S(2)}) collective-permute-start(bf16[512,128]{1,0:T(8,128)(2,1)} %get-tuple-element.56.rest_0_), channel_id=1, source_target_pairs={{0,4},{2,6},{4,0},{6,2},{1,5},{3,7},{5,1},{7,3},{8,12},{10,14},{12... | collective-permute-start | bytes 393224 | tf_op jit(solution)/shard_map/ppermute | solution.py:23
  106.5 11.6 %collective-permute-start.21 = (bf16[128,512]{1,0:T(8,128)(2,1)}, bf16[128,512]{1,0:T(8,128)(2,1)S(1)}, u32[]{:S(2)}, u32[]{:S(2)}) collective-permute-start(bf16[128,512]{1,0:T(8,128)(2,1)} %get-tuple-element.45.rest_0_), channel_id=1, source_target_pairs={{0,6},{2,4},{4,2},{6,0},{1,7},{3,5},{5,3},{7,1},{8,14},{10,12},{12... | collective-permute-start | bytes 393224 | tf_op jit(solution)/shard_map/ppermute | solution.py:23
  107.7 10.3 %collective-permute-start.20 = (bf16[128,512]{1,0:T(8,128)(2,1)}, bf16[128,512]{1,0:T(8,128)(2,1)S(1)}, u32[]{:S(2)}, u32[]{:S(2)}) collective-permute-start(bf16[128,512]{1,0:T(8,128)(2,1)} %get-tuple-element.45.rest_0_), channel_id=1, source_target_pairs={{0,4},{2,6},{4,0},{6,2},{1,5},{3,7},{5,1},{7,3},{8,12},{10,14},{12... | collective-permute-start | bytes 393224 | tf_op jit(solution)/shard_map/ppermute | solution.py:23
  108.7 9.4 %collective-permute-start.19 = (bf16[128,512]{1,0:T(8,128)(2,1)}, bf16[128,512]{1,0:T(8,128)(2,1)S(1)}, u32[]{:S(2)}, u32[]{:S(2)}) collective-permute-start(bf16[128,512]{1,0:T(8,128)(2,1)} %get-tuple-element.45.rest_0_), channel_id=1, source_target_pairs={{0,2},{2,0},{4,6},{6,4},{1,3},{3,1},{5,7},{7,5},{8,10},{10,8},{12,... | collective-permute-start | bytes 393224 | tf_op jit(solution)/shard_map/ppermute | solution.py:23
  (50 other events, 190.4 us)

commit v2 on v0

--- a/solution.py
+++ b/solution.py
@@ -1,11 +1,361 @@
 import jax
 import jax.numpy as jnp
 from jax import lax
+from jax.experimental import pallas as pl
+from jax.experimental.pallas import tpu as pltpu
 from jax.sharding import PartitionSpec as P
 
 BETA = 0.8
 RATE = 0.2
 EPS = 1e-06
+BF16 = jnp.bfloat16
+F32 = jnp.float32
+LIMIT = pltpu.CompilerParams(vmem_limit_bytes=16 * 2**20)
+HBM = pl.BlockSpec(memory_space=pltpu.HBM)
+GATHER = (0, 1, 2, 0)
+SMEM = pl.BlockSpec(memory_space=pltpu.SMEM)
+VMEM = pl.BlockSpec(memory_space=pltpu.VMEM)
+
+
+def far(x):
+    return pltpu.with_memory_space_constraint(x, pltpu.HBM)
+
+
+def flip(x, axis, m):
+    return lax.ppermute(x, axis, [(i, i ^ m) for i in range(lax.axis_size(axis))])
+
+
+def call(kernel, ids, args, outs, scratch=()):
+    return pl.pallas_call(
+        kernel,
+        out_shape=outs,
+        in_specs=[SMEM] + [VMEM] * len(args),
+        out_specs=jax.tree.map(lambda _: VMEM, outs),
+        scratch_shapes=scratch,
+        compiler_params=LIMIT,
+    )(ids, *args)
+
+
+def cut(ids, query_basis, output_basis, chunk, half):
+    def kernel(ids, query_basis, output_basis, out, sems):
+        at = (
+            pl.ds(pl.multiple_of(ids[1] * chunk, chunk), chunk),
+            pl.ds(pl.multiple_of(ids[2] * half, half), half),
+        )
+        copies = [
+            pltpu.make_async_copy(basis.at[at], out.at[pl.ds(i * chunk, chunk), :], sems.at[i])
+            for i, basis in enumerate((query_basis, output_basis))
+        ]
+        for copy in copies:
+            copy.start()
+        for copy in copies:
+            copy.wait()
+
+    return pl.pallas_call(
+        kernel,
+        out_shape=jax.ShapeDtypeStruct((2 * chunk, half), BF16),
+        in_specs=[SMEM, HBM, HBM],
+        out_specs=VMEM,
+        scratch_shapes=[pltpu.SemaphoreType.DMA((2,))],
+        compiler_params=LIMIT,
+    )(ids, far(query_basis), far(output_basis))
+
+
+def load(*arrays):
+    def kernel(*refs):
+        n = len(arrays)
+        copies = [
+            pltpu.make_async_copy(refs[i], refs[n + i], refs[2 * n].at[i]) for i in range(n)
+        ]
+        for copy in copies:
+            copy.start()
+        for copy in copies:
+            copy.wait()
+
+    return pl.pallas_call(
+        kernel,
+        out_shape=[jax.ShapeDtypeStruct(x.shape, x.dtype) for x in arrays],
+        in_specs=[HBM] * len(arrays),
+        out_specs=[VMEM] * len(arrays),
+        scratch_shapes=[pltpu.SemaphoreType.DMA((len(arrays),))],
+        compiler_params=LIMIT,
+    )(*map(far, arrays))
+
+
+def project(ids, tokens, bases, groups):
+    fs, reps = len(groups) + 1, len(groups[0])
+    rows = bases[0].shape[0]
+    chunk, half = rows // reps, groups[0][0].shape[1]
+    count = tokens[0].shape[0]
+    flat = [piece for group in groups for piece in group]
+
+    def kernel(ids, first, second, query_basis, output_basis, *rest):
+        pieces, out = rest[: len(flat)], rest[len(flat)]
+        f, r, t = ids[0], ids[1], ids[2]
+        for i, (x, basis) in enumerate(((first, query_basis), (second, output_basis))):
+            whole = rest[len(flat) + 1 + i]
+            whole[pl.ds(pl.multiple_of(f * rows, rows), rows), :] = basis[
+                :, pl.ds(pl.multiple_of(t * half, half), half)
+            ]
+            for k in range(1, fs):
+                for m in range(reps):
+                    at = (f ^ k) * rows + (r ^ m) * chunk
+                    whole[pl.ds(pl.multiple_of(at, chunk), chunk), :] = pieces[
+                        (k - 1) * reps + m
+                    ][i * chunk : (i + 1) * chunk, :]
+            out[i * count : (i + 1) * count, :] = jnp.dot(
+                x[...], whole[...], preferred_element_type=F32
+            ).astype(BF16)
+
+    return call(
+        kernel,
+        ids,
+        [*tokens, *bases, *flat],
+        jax.ShapeDtypeStruct((2 * count, half), BF16),
+        [pltpu.VMEM((fs * rows, half), BF16)] * 2,
+    )
+
+
+def contract(ids, mine, other, query_cot, attn_out, reps):
+    count, half = mine.shape[0] // 2, mine.shape[1]
+    rank, width = 2 * half, query_cot.shape[1]
+    share = rank // reps
+    tiles = width // share
+    shape = (2 * width, share)
+
+    def kernel(ids, mine, other, query_cot, attn_out, keep, *rest):
+        sends, both = rest[: reps - 1], rest[reps - 1]
+        r, t = ids[1], ids[2]
+        both[:, pl.ds(pl.multiple_of(t * half, half), half)] = mine[...]
+        both[:, pl.ds(pl.multiple_of((1 - t) * half, half), half)] = other[...]
+        for m in (*range(1, reps), 0):
+            out = sends[m - 1] if m else keep
+            ranks = pl.ds(pl.multiple_of((r ^ m) * share, share), share)
+            dims = (((0,), (0,)), ((), ()))
+            block = lax.dot_general(
+                both[:count, ranks], query_cot[...], dims, preferred_element_type=F32
+            ).astype(out.dtype)
+            for i in range(tiles):
+                out[i * share : (i + 1) * share, :] = block[:, i * share : (i + 1) * share]
+            out[width:, :] = lax.dot_general(
+                attn_out[...], both[count:, ranks], dims, preferred_element_type=F32
+            ).astype(out.dtype)
+
+    return call(
+        kernel,
+        ids,
+        [mine, other, query_cot, attn_out],
+        [jax.ShapeDtypeStruct(shape, F32)] + [jax.ShapeDtypeStruct(shape, BF16)] * (reps - 1),
+        [pltpu.VMEM((2 * count, rank), BF16)],
+    )
+
+
+def add_and_split(ids, keep, terms, fs):
+    rows, width = keep.shape
+    size = rows // (2 * fs)
+
+    def kernel(ids, keep, *rest):
+        terms, own, sends, total = rest[: -fs - 1], rest[-fs - 1], rest[-fs:-1], rest[-1]
+        f = ids[0]
+        value = keep[...]
+        for term in terms:
+            value = value + term[...].astype(F32)
+        total[...] = value
+        for k in (*range(1, fs), 0):
+            at = pl.multiple_of((f ^ k) * size, size)
+            out = sends[k - 1] if k else own
+            for i in range(2):
+                out[i * size : (i + 1) * size, :] = total[
+                    pl.ds(at + i * rows // 2, size), :
+                ].astype(out.dtype)
+
+    return call(
+        kernel,
+        ids,
+        [keep, *terms],
+        [jax.ShapeDtypeStruct((2 * size, width), F32)]
+        + [jax.ShapeDtypeStruct((2 * size, width), BF16)] * (fs - 1),
+        [pltpu.VMEM((rows, width), F32)],
+    )
+
+
+def total(ids, own, terms):
+    def kernel(ids, own, *rest):
+        value = own[...]
+        for term in rest[:-1]:
+            value = value + term[...].astype(F32)
+        rest[-1][...] = value.astype(BF16)
+
+    return call(kernel, ids, [own, *terms], jax.ShapeDtypeStruct(own.shape, BF16))
+
+
+def advance(ids, query_moment, output_moment, pieces):
+    fs = len(pieces)
+    size = output_moment.shape[0] // fs
+    moments = (query_moment, output_moment)
+
+    def kernel(ids, *rest):
+        olds, pieces, news, (rounded, squares) = rest[:2], rest[2:-4], rest[-4:-2], rest[-2:]
+        f = ids[0]
+        for i in range(2):
+            sums = jnp.zeros((8, pieces[0].shape[1]), F32)
+            for k, piece in enumerate(pieces):
+                start = pl.multiple_of((f ^ k) * size, size)
+                ds = pl.ds(start, size)
+                at = (slice(None), ds) if i == 0 else (ds, slice(None))
+                value = BETA * olds[i][at] + (1.0 - BETA) * piece[
+                    i * size : (i + 1) * size, :
+                ].astype(F32)
+                news[i][at] = value
+                rounded[pl.ds(start + i * fs * size, size), :] = value.astype(BF16)
+            value = news[i][...]
+            value = jnp.sum((value * value).reshape(value.shape[0] // 8, 8, value.shape[1]), axis=0)
+            for j in range(value.shape[1] // sums.shape[1]):
+                sums = sums + value[:, j * sums.shape[1] : (j + 1) * sums.shape[1]]
+            squares[8 * i : 8 * i + 8, :] = sums
+
+    return call(
+        kernel,
+        ids,
+        [*moments, *pieces],
+        [jax.ShapeDtypeStruct(x.shape, F32) for x in moments]
+        + [
+            jax.ShapeDtypeStruct((2 * fs * size, pieces[0].shape[1]), BF16),
+            jax.ShapeDtypeStruct((16, pieces[0].shape[1]), F32),
+        ],
+    )
+
+
+def finish(ids, squares, entries, bases, blocks, weights):
+    reps = len(blocks)
+    rows, width = weights[0].shape
+    rank = bases[0].shape[1]
+    share = rank // reps
+    tile = min(rows, 128)
+    steps = rows // tile
+
+    def kernel(ids, *rest):
+        squares, query_basis, output_basis, *rest = rest
+        blocks, rest = rest[:reps], rest[reps:]
+        weights, outs, kept, (query_whole, output_whole, sems) = (
+            rest[:2],
+            rest[2:8],
+            rest[8:14],
+            rest[14:],
+        )
+        r = ids[1]
+        for m in range(reps):
+            at = pl.ds(pl.multiple_of((r ^ m) * share, share), share)
+            for i in range(width // share):
+                cols = slice(i * share, (i + 1) * share)
+                query_whole[at, cols] = blocks[m][cols, :]
+            output_whole[:, at] = blocks[m][width:, :]
+        value = squares[...]
+        copies = []
+        for i in range(2):
+            scale = lax.rsqrt(jnp.sum(value[8 * i : 8 * i + 8, :]) * (1.0 / entries) + EPS)
+            for j in range(steps):
+                at = slice(j * tile, (j + 1) * tile)
+                if i == 0:
+                    step = jnp.dot(
+                        query_basis[at, :], query_whole[...], preferred_element_type=F32
+                    )
+                else:
+                    step = lax.dot_general(
+                        output_whole[at, :],
+                        output_basis[...],
+                        (((1,), (1,)), ((), ())),
+                        preferred_element_type=F32,
+                    )
+                step = step * scale
+                new = weights[i][at, :] - RATE * step
+                for n, result in enumerate((step, new, new.astype(BF16))):
+                    n = 3 * i + n
+                    kept[n][at, :] = result
+                    copies.append(
+                        pltpu.make_async_copy(
+                            kept[n].at[at, :], outs[n].at[at, :], sems.at[n * steps + j]
+                        )
+                    )
+                    copies[-1].start()
+        for copy in copies:
+            copy.wait()
+
+    kinds = (F32, F32, BF16) * 2
+    args = [squares, *bases, *blocks, *weights]
+    return pl.pallas_call(
+        kernel,
+        out_shape=[jax.ShapeDtypeStruct((rows, width), kind) for kind in kinds],
+        in_specs=[SMEM] + [VMEM] * len(args),
+        out_specs=[HBM] * 6,
+        scratch_shapes=[pltpu.VMEM((rows, width), kind) for kind in kinds]
+        + [
+            pltpu.VMEM((rank, width), BF16),
+            pltpu.VMEM((rows, rank), BF16),
+            pltpu.SemaphoreType.DMA((6 * steps,)),
+        ],
+        compiler_params=LIMIT,
+    )(ids, *args)
+
+
+def gather(x, fewer):
+    one, two = flip(x, "rep", 1), flip(x, "rep", 2)
+    if fewer == 1:
+        return [x, one, two, flip(one, "rep", 2)]
+    if fewer == 2:
+        return [x, one, two, flip(two, "rep", 1)]
+    return [x, one, two, flip(x, "rep", 3)]
+
+
+def direct(
+    saved_input,
+    query_cot,
+    attn_out,
+    out_cot,
+    query_basis,
+    output_basis,
+    query_weight,
+    output_weight,
+    query_moment,
+    output_moment,
+):
+    fs, reps, tps = (lax.axis_size(axis) for axis in ("fs", "rep", "tp"))
+    ids = jnp.stack([lax.axis_index(axis) for axis in ("fs", "rep", "tp")]).astype(jnp.int32)
+    rows, rank = query_basis.shape
+    piece = cut(ids, query_basis, output_basis, rows // reps, rank // tps)
+    groups = [gather(flip(piece, "fs", k), GATHER[k]) for k in range(1, fs)]
+    tokens = load(saved_input, out_cot)
+    mine = project(ids, tokens, (query_basis, output_basis), groups)
+    keep, *sends = contract(ids, mine, flip(mine, "tp", 1), query_cot, attn_out, reps)
+    terms = [flip(send, "rep", m + 1) for m, send in enumerate(sends)]
+    own, *sends = add_and_split(ids, keep, terms, fs)
+    part = total(ids, own, [flip(send, "fs", k + 1) for k, send in enumerate(sends)])
+    pieces = [part] + [flip(part, "fs", k) for k in range(1, fs)]
+    query_moment_new, output_moment_new, rounded, squares = advance(
+        ids, query_moment, output_moment, pieces
+    )
+    blocks = gather(rounded, 0)
+    squares = squares + flip(squares, "tp", 1)
+    squares = squares + flip(squares, "rep", 1)
+    squares = squares + flip(squares, "rep", 2)
+    query_step, query_new, query_copy, output_step, output_new, output_copy = finish(
+        ids,
+        squares,
+        query_moment.size * reps * tps,
+        (query_basis, output_basis),
+        blocks,
+        (query_weight, output_weight),
+    )
+    return (
+        query_step,
+        output_step,
+        query_new,
+        output_new,
+        query_copy,
+        output_copy,
+        query_moment_new,
+        output_moment_new,
+    )
 
 
 def on_device(
@@ -98,8 +448,9 @@
         P("rep", "tp"),
         P("tp", "rep"),
     )
+    small = mesh.shape["fs"] == 4 and mesh.shape["rep"] == 4 and mesh.shape["tp"] == 2
     return jax.shard_map(
-        on_device,
+        direct if small else on_device,
         mesh=mesh,
         in_specs=placed,
         out_specs=(

time: 254 us -> 91.5 us (0.36)
  waiting for transfers between devices: 157 us -> 42.7 us
  blocking collectives: 32.6 us -> 0 us
  starting transfers between devices: 7.38 us -> 35 us
  matrix products: 16.3 us -> 0 us
  local copies, waits for them, and re-layouts: 15.8 us -> 0.05 us
  between operations: 15.2 us -> 0.82 us
  Pallas kernels: 0 us -> 12.6 us
  other arithmetic: 8.72 us -> 0.09 us
    reduce_scatter x1 -> x0, waiting for transfers between devices: 69.5 us -> none  [on_device(): lax.psum_scatter(jnp.dot(saved_input.T, query_cot, preferred_element_type...]
    all_gather x1 -> x0, waiting for transfers between devices: 45.2 us -> none  [on_device(): lax.all_gather(output_basis, 'fs', axis=0, tiled=True)]
    ppermute x0 -> x28, waiting for transfers between devices: none -> 42.7 us  [flip(): lax.ppermute(x, axis, [(i, i ^ m) for i in range(lax.axis_size(axis))])]
    ppermute x0 -> x28, starting transfers between devices: none -> 35 us  [flip(): lax.ppermute(x, axis, [(i, i ^ m) for i in range(lax.axis_size(axis))])]
    psum x1 -> x0, waiting for transfers between devices: 34.8 us -> none  [on_device(): query_share, output_flip = lax.psum((query_local, output_local), 'fs')]
    all_gather x2 -> x0, blocking collectives: 19.3 us -> none  [the longest x1 10.2 us: on_device(): lax.all_gather(query_dir, 'rep', axis=0, tiled=True)]
    dot_general x6 -> x0, matrix products: 16.3 us -> none  [the longest x1 4.22 us: on_device(): jnp.dot(saved_input.T, query_cot, preferred_element_type=jnp.float32)]
    unnamed x29 -> x16, local copies, waits for them, and re-layouts: 14.5 us -> 0.05 us
  transfers between devices with their start and end apart: 5 -> 28, of which waited for: 4 -> 16; matrix products, arithmetic and copies ran while one was open for 7% -> 0% of each run, Pallas kernels for 0% -> 2%
where the time goes in v2:
time: 91.5 us; the launch traced here: 91.3 us
  waiting for transfers between devices  42.7 us (47%)
  starting transfers between devices  35 us (38%)
  Pallas kernels  12.6 us (14%)
    ppermute x28, waiting for transfers between devices, flip(): lax.ppermute(x, axis, [(i, i ^ m) for i in range(lax.axis_size(axis))])  42.7 us
    ppermute x28, starting transfers between devices, flip(): lax.ppermute(x, axis, [(i, i ^ m) for i in range(lax.axis_size(axis))])  35 us
    pallas_call x5, Pallas kernels, call(): pl.pallas_call(kernel, out_shape=outs, in_specs=[SMEM] + [VMEM] * len(arg...  5.88 us
    pallas_call x1, Pallas kernels, finish(): pl.pallas_call(kernel, out_shape=[jax.ShapeDtypeStruct((rows, width), kin...  3.42 us
  transfers between devices with their start and end apart: 28, of which 16 were waited for; matrix products, arithmetic and copies ran while one was open for 0% of the time, Pallas kernels for 2%

profile of v2, /device:TPU:0, one launch (start us, length us, event | category | flops | bytes accessed | tf_op | source)
XLA Modules:
  0.0 91.3 jit_solution(12234230724288201686)
XLA Ops:
  2.2 5.1 %collective-permute-start.8 = (bf16[256,256]{1,0:T(8,128)(2,1)S(1)}, bf16[256,256]{1,0:T(8,128)(2,1)S(1)}, u32[]{:S(2)}, u32[]{:S(2)}) collective-permute-start(bf16[256,256]{1,0:T(8,128)(2,1)S(1)} %shard_map.162), channel_id=1, source_target_pairs={{0,24},{8,16},{16,8},{24,0},{1,25},{9,17},{17,9},{25,1},{2,26},{10... | collective-permute-start | bytes 393224 | tf_op jit(solution)/shard_map/ppermute | solution.py:25
  8.0 3.8 %collective-permute-done.8.rest_8_ = bf16[256,256]{1,0:T(8,128)(2,1)S(1)} collective-permute-done((bf16[256,256]{1,0:T(8,128)(2,1)S(1)}, bf16[256,256]{1,0:T(8,128)(2,1)S(1)}, u32[]{:S(2)}, u32[]{:S(2)}) %collective-permute-start.8) | collective-permute-done | bytes 131104 | tf_op jit(solution)/shard_map/ppermute | solution.py:25
  11.8 2.6 %collective-permute-start.11 = (bf16[256,256]{1,0:T(8,128)(2,1)S(1)}, bf16[256,256]{1,0:T(8,128)(2,1)S(1)}, u32[]{:S(2)}, u32[]{:S(2)}) collective-permute-start(bf16[256,256]{1,0:T(8,128)(2,1)S(1)} %collective-permute-done.8.rest_8_), channel_id=1, source_target_pairs={{0,6},{2,4},{4,2},{6,0},{1,7},{3,5},{5,3},{7,1},{8,14},{10,12},{12... | collective-permute-start | bytes 393224 | tf_op jit(solution)/shard_map/ppermute | solution.py:25
  14.9 3.5 %collective-permute-done.4.rest_4_ = bf16[256,256]{1,0:T(8,128)(2,1)S(1)} collective-permute-done((bf16[256,256]{1,0:T(8,128)(2,1)S(1)}, bf16[256,256]{1,0:T(8,128)(2,1)S(1)}, u32[]{:S(2)}, u32[]{:S(2)}) %collective-permute-start.4) | collective-permute-done | bytes 131104 | tf_op jit(solution)/shard_map/ppermute | solution.py:25
  18.4 1.5 %collective-permute-start.6 = (bf16[256,256]{1,0:T(8,128)(2,1)S(1)}, bf16[256,256]{1,0:T(8,128)(2,1)S(1)}, u32[]{:S(2)}, u32[]{:S(2)}) collective-permute-start(bf16[256,256]{1,0:T(8,128)(2,1)S(1)} %collective-permute-done.4.rest_4_), channel_id=1, source_target_pairs={{0,4},{2,6},{4,0},{6,2},{1,5},{3,7},{5,1},{7,3},{8,12},{10,14},{12... | collective-permute-start | bytes 393224 | tf_op jit(solution)/shard_map/ppermute | solution.py:25
  27.6 1.8 %shard_map.161 = (bf16[352,2048]{1,0:T(8,128)(2,1)S(1)}, bf16[352,2048]{1,0:T(8,128)(2,1)S(1)}) custom-call(bf16[352,2048]{1,0:T(8,128)(2,1)} %refs_0_.1, bf16[352,2048]{1,0:T(8,128)(2,1)} %refs_1_.1), custom_call_target="tpu_custom_call" | custom-call | tf_op jit(solution)/shard_map/pallas_call | solution.py:75
  29.5 1.8 %collective-permute-done.5.rest_5_ = bf16[256,256]{1,0:T(8,128)(2,1)S(1)} collective-permute-done((bf16[256,256]{1,0:T(8,128)(2,1)S(1)}, bf16[256,256]{1,0:T(8,128)(2,1)S(1)}, u32[]{:S(2)}, u32[]{:S(2)}) %collective-permute-start.5) | collective-permute-done | bytes 131104 | tf_op jit(solution)/shard_map/ppermute | solution.py:25
  32.7 1.6 %shard_map.163.mine = bf16[704,256]{1,0:T(8,128)(2,1)S(1)} custom-call(s32[3]{0:T(128)S(1)} %pad_add_fusion.ids, bf16[352,2048]{1,0:T(8,128)(2,1)S(1)} %get-tuple-element.28.first, bf16[352,2048]{1,0:T(8,128)(2,1)S(1)} %get-tuple-element.29.second, bf16[512,512]{1,0:T(8,128)(2,1)S(1)} %copy-done, bf16[512,512]{1,0:T(8,128)(2,1)S(1)} %copy-done.1, ...), custom_call_target="tpu_custom_call" | custom-call | tf_op jit(solution)/shard_map/pallas_call | solution.py:29
  34.4 1.7 %collective-permute-done.12.other = bf16[704,256]{1,0:T(8,128)(2,1)S(1)} collective-permute-done((bf16[704,256]{1,0:T(8,128)(2,1)S(1)}, bf16[704,256]{1,0:T(8,128)(2,1)S(1)}, u32[]{:S(2)}, u32[]{:S(2)}) %collective-permute-start.12) | collective-permute-done | bytes 360480 | tf_op jit(solution)/shard_map/ppermute | solution.py:25
  36.1 1.5 %shard_map.164 = (f32[1024,128]{1,0:T(8,128)S(1)}, bf16[1024,128]{1,0:T(8,128)(2,1)S(1)}, bf16[1024,128]{1,0:T(8,128)(2,1)S(1)}, bf16[1024,128]{1,0:T(8,128)(2,1)S(1)}) custom-call(s32[3]{0:T(128)S(1)} %pad_add_fusion.ids, bf16[704,256]{1,0:T(8,128)(2,1)S(1)} %shard_map.163.mine, bf16[704,256]{1,0:T(8,128)(2,1)S(1)} %collective-permute-done.12.other, ...), custom_call_target="tpu_custom_call" | custom-call | tf_op jit(solution)/shard_map/pallas_call | solution.py:29
  37.6 1.6 %collective-permute-start.13 = (bf16[1024,128]{1,0:T(8,128)(2,1)S(1)}, bf16[1024,128]{1,0:T(8,128)(2,1)S(1)}, u32[]{:S(2)}, u32[]{:S(2)}) collective-permute-start(bf16[1024,128]{1,0:T(8,128)(2,1)S(1)} %get-tuple-element.31), channel_id=1, source_target_pairs={{0,2},{2,0},{4,6},{6,4},{1,3},{3,1},{5,7},{7,5},{8,10},{10,8},{12,... | collective-permute-start | bytes 786440 | tf_op jit(solution)/shard_map/ppermute | solution.py:25
  41.1 5.7 %collective-permute-done.13.rest_0_ = bf16[1024,128]{1,0:T(8,128)(2,1)S(1)} collective-permute-done((bf16[1024,128]{1,0:T(8,128)(2,1)S(1)}, bf16[1024,128]{1,0:T(8,128)(2,1)S(1)}, u32[]{:S(2)}, u32[]{:S(2)}) %collective-permute-start.13) | collective-permute-done | bytes 262176 | tf_op jit(solution)/shard_map/ppermute | solution.py:25
  46.8 6.0 %collective-permute-done.14.rest_1_ = bf16[1024,128]{1,0:T(8,128)(2,1)S(1)} collective-permute-done((bf16[1024,128]{1,0:T(8,128)(2,1)S(1)}, bf16[1024,128]{1,0:T(8,128)(2,1)S(1)}, u32[]{:S(2)}, u32[]{:S(2)}) %collective-permute-start.14) | collective-permute-done | bytes 262176 | tf_op jit(solution)/shard_map/ppermute | solution.py:25
  53.6 1.6 %collective-permute-start.16 = (bf16[256,128]{1,0:T(8,128)(2,1)S(1)}, bf16[256,128]{1,0:T(8,128)(2,1)S(1)}, u32[]{:S(2)}, u32[]{:S(2)}) collective-permute-start(bf16[256,128]{1,0:T(8,128)(2,1)S(1)} %get-tuple-element.35), channel_id=1, source_target_pairs={{0,8},{8,0},{16,24},{24,16},{1,9},{9,1},{17,25},{25,17},{2,10},{10... | collective-permute-start | bytes 196616 | tf_op jit(solution)/shard_map/ppermute | solution.py:25
  55.2 1.6 %collective-permute-start.17 = (bf16[256,128]{1,0:T(8,128)(2,1)S(1)}, bf16[256,128]{1,0:T(8,128)(2,1)S(1)}, u32[]{:S(2)}, u32[]{:S(2)}) collective-permute-start(bf16[256,128]{1,0:T(8,128)(2,1)S(1)} %get-tuple-element.36), channel_id=1, source_target_pairs={{0,16},{8,24},{16,0},{24,8},{1,17},{9,25},{17,1},{25,9},{2,18},{10... | collective-permute-start | bytes 196616 | tf_op jit(solution)/shard_map/ppermute | solution.py:25
  58.6 3.2 %collective-permute-done.17.rest_1_ = bf16[256,128]{1,0:T(8,128)(2,1)S(1)} collective-permute-done((bf16[256,128]{1,0:T(8,128)(2,1)S(1)}, bf16[256,128]{1,0:T(8,128)(2,1)S(1)}, u32[]{:S(2)}, u32[]{:S(2)}) %collective-permute-start.17) | collective-permute-done | bytes 65568 | tf_op jit(solution)/shard_map/ppermute | solution.py:25
  63.4 2.1 %collective-permute-start.21 = (bf16[256,128]{1,0:T(8,128)(2,1)S(1)}, bf16[256,128]{1,0:T(8,128)(2,1)S(1)}, u32[]{:S(2)}, u32[]{:S(2)}) collective-permute-start(bf16[256,128]{1,0:T(8,128)(2,1)S(1)} %shard_map.166.rest_2_), channel_id=1, source_target_pairs={{0,24},{8,16},{16,8},{24,0},{1,25},{9,17},{17,9},{25,1},{2,26},{10... | collective-permute-start | bytes 196616 | tf_op jit(solution)/shard_map/ppermute | solution.py:25
  65.9 2.0 %collective-permute-start.19 = (bf16[256,128]{1,0:T(8,128)(2,1)S(1)}, bf16[256,128]{1,0:T(8,128)(2,1)S(1)}, u32[]{:S(2)}, u32[]{:S(2)}) collective-permute-start(bf16[256,128]{1,0:T(8,128)(2,1)S(1)} %shard_map.166.rest_2_), channel_id=1, source_target_pairs={{0,8},{8,0},{16,24},{24,16},{1,9},{9,1},{17,25},{25,17},{2,10},{10... | collective-permute-start | bytes 196616 | tf_op jit(solution)/shard_map/ppermute | solution.py:25
  67.9 1.8 %collective-permute-done.21.rest_5_ = bf16[256,128]{1,0:T(8,128)(2,1)S(1)} collective-permute-done((bf16[256,128]{1,0:T(8,128)(2,1)S(1)}, bf16[256,128]{1,0:T(8,128)(2,1)S(1)}, u32[]{:S(2)}, u32[]{:S(2)}) %collective-permute-start.21) | collective-permute-done | bytes 65568 | tf_op jit(solution)/shard_map/ppermute | solution.py:25
  69.7 1.5 %collective-permute-done.20.rest_4_ = bf16[256,128]{1,0:T(8,128)(2,1)S(1)} collective-permute-done((bf16[256,128]{1,0:T(8,128)(2,1)S(1)}, bf16[256,128]{1,0:T(8,128)(2,1)S(1)}, u32[]{:S(2)}, u32[]{:S(2)}) %collective-permute-start.20) | collective-permute-done | bytes 65568 | tf_op jit(solution)/shard_map/ppermute | solution.py:25
  72.6 1.7 %collective-permute-start.27 = (bf16[1024,128]{1,0:T(8,128)(2,1)S(1)}, bf16[1024,128]{1,0:T(8,128)(2,1)S(1)}, u32[]{:S(2)}, u32[]{:S(2)}) collective-permute-start(bf16[1024,128]{1,0:T(8,128)(2,1)S(1)} %get-tuple-element.39.rest_3_), channel_id=1, source_target_pairs={{0,6},{2,4},{4,2},{6,0},{1,7},{3,5},{5,3},{7,1},{8,14},{10,12},{12... | collective-permute-start | bytes 786440 | tf_op jit(solution)/shard_map/ppermute | solution.py:25
  78.5 5.6 %collective-permute-done.23 = f32[16,128]{1,0:T(8,128)S(1)} collective-permute-done((f32[16,128]{1,0:T(8,128)S(1)}, f32[16,128]{1,0:T(8,128)S(1)}, u32[]{:S(2)}, u32[]{:S(2)}) %collective-permute-start.23) | collective-permute-done | bytes 8224 | tf_op jit(solution)/shard_map/ppermute | solution.py:25
  84.8 3.0 %collective-permute-done.24 = f32[16,128]{1,0:T(8,128)S(1)} collective-permute-done((f32[16,128]{1,0:T(8,128)S(1)}, f32[16,128]{1,0:T(8,128)S(1)}, u32[]{:S(2)}, u32[]{:S(2)}) %collective-permute-start.24) | collective-permute-done | bytes 8224 | tf_op jit(solution)/shard_map/ppermute | solution.py:25
  87.8 3.4 %shard_map.168 = (f32[512,512]{1,0:T(8,128)}, f32[512,512]{1,0:T(8,128)}, bf16[512,512]{1,0:T(8,128)(2,1)}, f32[512,512]{1,0:T(8,128)}, f32[512,512]{1,0:T(8,128)}, /*index=5*/bf16[512,512]{1,0:T(8,128)(2,1)}) custom-call(s32[3]{0:T(128)S(1)} %pad_add_fusion.ids, f32[16,128]{1,0:T(8,128)S(1)} %add.11.rest_0_, bf16[512,512]{1,0:T(8,128)(2,1)S(1)} %copy-done, ...), custom_call_target="tpu_custom_call" | custom-call | tf_op jit(solution)/shard_map/pallas_call | solution.py:286
  (60 shorter events, 24.8 us)
Async XLA Ops:
  2.2 9.6 %collective-permute-start.8 = (bf16[256,256]{1,0:T(8,128)(2,1)S(1)}, bf16[256,256]{1,0:T(8,128)(2,1)S(1)}, u32[]{:S(2)}, u32[]{:S(2)}) collective-permute-start(bf16[256,256]{1,0:T(8,128)(2,1)S(1)} %shard_map.162), channel_id=1, source_target_pairs={{0,24},{8,16},{16,8},{24,0},{1,25},{9,17},{17,9},{25,1},{2,26},{10... | collective-permute-start | bytes 393224 | tf_op jit(solution)/shard_map/ppermute | solution.py:25
  7.3 11.1 %collective-permute-start.4 = (bf16[256,256]{1,0:T(8,128)(2,1)S(1)}, bf16[256,256]{1,0:T(8,128)(2,1)S(1)}, u32[]{:S(2)}, u32[]{:S(2)}) collective-permute-start(bf16[256,256]{1,0:T(8,128)(2,1)S(1)} %shard_map.162), channel_id=1, source_target_pairs={{0,16},{8,24},{16,0},{24,8},{1,17},{9,25},{17,1},{25,9},{2,18},{10... | collective-permute-start | bytes 393224 | tf_op jit(solution)/shard_map/ppermute | solution.py:25
  7.3 12.6 %collective-permute-start = (bf16[256,256]{1,0:T(8,128)(2,1)S(1)}, bf16[256,256]{1,0:T(8,128)(2,1)S(1)}, u32[]{:S(2)}, u32[]{:S(2)}) collective-permute-start(bf16[256,256]{1,0:T(8,128)(2,1)S(1)} %shard_map.162), channel_id=1, source_target_pairs={{0,8},{8,0},{16,24},{24,16},{1,9},{9,1},{17,25},{25,17},{2,10},{10... | collective-permute-start | bytes 393224 | tf_op jit(solution)/shard_map/ppermute | solution.py:25
  11.8 10.2 %collective-permute-start.11 = (bf16[256,256]{1,0:T(8,128)(2,1)S(1)}, bf16[256,256]{1,0:T(8,128)(2,1)S(1)}, u32[]{:S(2)}, u32[]{:S(2)}) collective-permute-start(bf16[256,256]{1,0:T(8,128)(2,1)S(1)} %collective-permute-done.8.rest_8_), channel_id=1, source_target_pairs={{0,6},{2,4},{4,2},{6,0},{1,7},{3,5},{5,3},{7,1},{8,14},{10,12},{12... | collective-permute-start | bytes 393224 | tf_op jit(solution)/shard_map/ppermute | solution.py:25
  14.4 9.1 %collective-permute-start.10 = (bf16[256,256]{1,0:T(8,128)(2,1)S(1)}, bf16[256,256]{1,0:T(8,128)(2,1)S(1)}, u32[]{:S(2)}, u32[]{:S(2)}) collective-permute-start(bf16[256,256]{1,0:T(8,128)(2,1)S(1)} %collective-permute-done.8.rest_8_), channel_id=1, source_target_pairs={{0,4},{2,6},{4,0},{6,2},{1,5},{3,7},{5,1},{7,3},{8,12},{10,14},{12... | collective-permute-start | bytes 393224 | tf_op jit(solution)/shard_map/ppermute | solution.py:25
  18.4 5.6 %collective-permute-start.6 = (bf16[256,256]{1,0:T(8,128)(2,1)S(1)}, bf16[256,256]{1,0:T(8,128)(2,1)S(1)}, u32[]{:S(2)}, u32[]{:S(2)}) collective-permute-start(bf16[256,256]{1,0:T(8,128)(2,1)S(1)} %collective-permute-done.4.rest_4_), channel_id=1, source_target_pairs={{0,4},{2,6},{4,0},{6,2},{1,5},{3,7},{5,1},{7,3},{8,12},{10,14},{12... | collective-permute-start | bytes 393224 | tf_op jit(solution)/shard_map/ppermute | solution.py:25
  19.9 6.4 %collective-permute-start.1 = (bf16[256,256]{1,0:T(8,128)(2,1)S(1)}, bf16[256,256]{1,0:T(8,128)(2,1)S(1)}, u32[]{:S(2)}, u32[]{:S(2)}) collective-permute-start(bf16[256,256]{1,0:T(8,128)(2,1)S(1)} %collective-permute-done.rest_0_), channel_id=1, source_target_pairs={{0,2},{2,0},{4,6},{6,4},{1,3},{3,1},{5,7},{7,5},{8,10},{10,8},{12,... | collective-permute-start | bytes 393224 | tf_op jit(solution)/shard_map/ppermute | solution.py:25
  21.4 8.0 %collective-permute-start.9 = (bf16[256,256]{1,0:T(8,128)(2,1)S(1)}, bf16[256,256]{1,0:T(8,128)(2,1)S(1)}, u32[]{:S(2)}, u32[]{:S(2)}) collective-permute-start(bf16[256,256]{1,0:T(8,128)(2,1)S(1)} %collective-permute-done.8.rest_8_), channel_id=1, source_target_pairs={{0,2},{2,0},{4,6},{6,4},{1,3},{3,1},{5,7},{7,5},{8,10},{10,8},{12,... | collective-permute-start | bytes 393224 | tf_op jit(solution)/shard_map/ppermute | solution.py:25
  22.0 9.3 %collective-permute-start.5 = (bf16[256,256]{1,0:T(8,128)(2,1)S(1)}, bf16[256,256]{1,0:T(8,128)(2,1)S(1)}, u32[]{:S(2)}, u32[]{:S(2)}) collective-permute-start(bf16[256,256]{1,0:T(8,128)(2,1)S(1)} %collective-permute-done.4.rest_4_), channel_id=1, source_target_pairs={{0,2},{2,0},{4,6},{6,4},{1,3},{3,1},{5,7},{7,5},{8,10},{10,8},{12,... | collective-permute-start | bytes 393224 | tf_op jit(solution)/shard_map/ppermute | solution.py:25
  23.4 7.8 %collective-permute-start.2 = (bf16[256,256]{1,0:T(8,128)(2,1)S(1)}, bf16[256,256]{1,0:T(8,128)(2,1)S(1)}, u32[]{:S(2)}, u32[]{:S(2)}) collective-permute-start(bf16[256,256]{1,0:T(8,128)(2,1)S(1)} %collective-permute-done.rest_0_), channel_id=1, source_target_pairs={{0,4},{2,6},{4,0},{6,2},{1,5},{3,7},{5,1},{7,3},{8,12},{10,14},{12... | collective-permute-start | bytes 393224 | tf_op jit(solution)/shard_map/ppermute | solution.py:25
  24.0 8.7 %collective-permute-start.7 = (bf16[256,256]{1,0:T(8,128)(2,1)S(1)}, bf16[256,256]{1,0:T(8,128)(2,1)S(1)}, u32[]{:S(2)}, u32[]{:S(2)}) collective-permute-start(bf16[256,256]{1,0:T(8,128)(2,1)S(1)} %collective-permute-done.6.rest_6_), channel_id=1, source_target_pairs={{0,2},{2,0},{4,6},{6,4},{1,3},{3,1},{5,7},{7,5},{8,10},{10,8},{12,... | collective-permute-start | bytes 393224 | tf_op jit(solution)/shard_map/ppermute | solution.py:25
  26.3 6.3 %collective-permute-start.3 = (bf16[256,256]{1,0:T(8,128)(2,1)S(1)}, bf16[256,256]{1,0:T(8,128)(2,1)S(1)}, u32[]{:S(2)}, u32[]{:S(2)}) collective-permute-start(bf16[256,256]{1,0:T(8,128)(2,1)S(1)} %collective-permute-done.1.rest_1_), channel_id=1, source_target_pairs={{0,4},{2,6},{4,0},{6,2},{1,5},{3,7},{5,1},{7,3},{8,12},{10,14},{12... | collective-permute-start | bytes 393224 | tf_op jit(solution)/shard_map/ppermute | solution.py:25
  37.6 9.2 %collective-permute-start.13 = (bf16[1024,128]{1,0:T(8,128)(2,1)S(1)}, bf16[1024,128]{1,0:T(8,128)(2,1)S(1)}, u32[]{:S(2)}, u32[]{:S(2)}) collective-permute-start(bf16[1024,128]{1,0:T(8,128)(2,1)S(1)} %get-tuple-element.31), channel_id=1, source_target_pairs={{0,2},{2,0},{4,6},{6,4},{1,3},{3,1},{5,7},{7,5},{8,10},{10,8},{12,... | collective-permute-start | bytes 786440 | tf_op jit(solution)/shard_map/ppermute | solution.py:25
  39.1 13.7 %collective-permute-start.14 = (bf16[1024,128]{1,0:T(8,128)(2,1)S(1)}, bf16[1024,128]{1,0:T(8,128)(2,1)S(1)}, u32[]{:S(2)}, u32[]{:S(2)}) collective-permute-start(bf16[1024,128]{1,0:T(8,128)(2,1)S(1)} %get-tuple-element.32), channel_id=1, source_target_pairs={{0,4},{2,6},{4,0},{6,2},{1,5},{3,7},{5,1},{7,3},{8,12},{10,14},{12... | collective-permute-start | bytes 786440 | tf_op jit(solution)/shard_map/ppermute | solution.py:25
  39.6 13.2 %collective-permute-start.15 = (bf16[1024,128]{1,0:T(8,128)(2,1)S(1)}, bf16[1024,128]{1,0:T(8,128)(2,1)S(1)}, u32[]{:S(2)}, u32[]{:S(2)}) collective-permute-start(bf16[1024,128]{1,0:T(8,128)(2,1)S(1)} %get-tuple-element.33), channel_id=1, source_target_pairs={{0,6},{2,4},{4,2},{6,0},{1,7},{3,5},{5,3},{7,1},{8,14},{10,12},{12... | collective-permute-start | bytes 786440 | tf_op jit(solution)/shard_map/ppermute | solution.py:25
  55.2 6.6 %collective-permute-start.17 = (bf16[256,128]{1,0:T(8,128)(2,1)S(1)}, bf16[256,128]{1,0:T(8,128)(2,1)S(1)}, u32[]{:S(2)}, u32[]{:S(2)}) collective-permute-start(bf16[256,128]{1,0:T(8,128)(2,1)S(1)} %get-tuple-element.36), channel_id=1, source_target_pairs={{0,16},{8,24},{16,0},{24,8},{1,17},{9,25},{17,1},{25,9},{2,18},{10... | collective-permute-start | bytes 196616 | tf_op jit(solution)/shard_map/ppermute | solution.py:25
  56.8 6.1 %collective-permute-start.18 = (bf16[256,128]{1,0:T(8,128)(2,1)S(1)}, bf16[256,128]{1,0:T(8,128)(2,1)S(1)}, u32[]{:S(2)}, u32[]{:S(2)}) collective-permute-start(bf16[256,128]{1,0:T(8,128)(2,1)S(1)} %get-tuple-element.37), channel_id=1, source_target_pairs={{0,24},{8,16},{16,8},{24,0},{1,25},{9,17},{17,9},{25,1},{2,26},{10... | collective-permute-start | bytes 196616 | tf_op jit(solution)/shard_map/ppermute | solution.py:25
  63.4 6.2 %collective-permute-start.21 = (bf16[256,128]{1,0:T(8,128)(2,1)S(1)}, bf16[256,128]{1,0:T(8,128)(2,1)S(1)}, u32[]{:S(2)}, u32[]{:S(2)}) collective-permute-start(bf16[256,128]{1,0:T(8,128)(2,1)S(1)} %shard_map.166.rest_2_), channel_id=1, source_target_pairs={{0,24},{8,16},{16,8},{24,0},{1,25},{9,17},{17,9},{25,1},{2,26},{10... | collective-permute-start | bytes 196616 | tf_op jit(solution)/shard_map/ppermute | solution.py:25
  65.5 5.7 %collective-permute-start.20 = (bf16[256,128]{1,0:T(8,128)(2,1)S(1)}, bf16[256,128]{1,0:T(8,128)(2,1)S(1)}, u32[]{:S(2)}, u32[]{:S(2)}) collective-permute-start(bf16[256,128]{1,0:T(8,128)(2,1)S(1)} %shard_map.166.rest_2_), channel_id=1, source_target_pairs={{0,16},{8,24},{16,0},{24,8},{1,17},{9,25},{17,1},{25,9},{2,18},{10... | collective-permute-start | bytes 196616 | tf_op jit(solution)/shard_map/ppermute | solution.py:25
  65.9 5.3 %collective-permute-start.19 = (bf16[256,128]{1,0:T(8,128)(2,1)S(1)}, bf16[256,128]{1,0:T(8,128)(2,1)S(1)}, u32[]{:S(2)}, u32[]{:S(2)}) collective-permute-start(bf16[256,128]{1,0:T(8,128)(2,1)S(1)} %shard_map.166.rest_2_), channel_id=1, source_target_pairs={{0,8},{8,0},{16,24},{24,16},{1,9},{9,1},{17,25},{25,17},{2,10},{10... | collective-permute-start | bytes 196616 | tf_op jit(solution)/shard_map/ppermute | solution.py:25
  72.6 15.2 %collective-permute-start.27 = (bf16[1024,128]{1,0:T(8,128)(2,1)S(1)}, bf16[1024,128]{1,0:T(8,128)(2,1)S(1)}, u32[]{:S(2)}, u32[]{:S(2)}) collective-permute-start(bf16[1024,128]{1,0:T(8,128)(2,1)S(1)} %get-tuple-element.39.rest_3_), channel_id=1, source_target_pairs={{0,6},{2,4},{4,2},{6,0},{1,7},{3,5},{5,3},{7,1},{8,14},{10,12},{12... | collective-permute-start | bytes 786440 | tf_op jit(solution)/shard_map/ppermute | solution.py:25
  74.3 13.5 %collective-permute-start.26 = (bf16[1024,128]{1,0:T(8,128)(2,1)S(1)}, bf16[1024,128]{1,0:T(8,128)(2,1)S(1)}, u32[]{:S(2)}, u32[]{:S(2)}) collective-permute-start(bf16[1024,128]{1,0:T(8,128)(2,1)S(1)} %get-tuple-element.39.rest_3_), channel_id=1, source_target_pairs={{0,4},{2,6},{4,0},{6,2},{1,5},{3,7},{5,1},{7,3},{8,12},{10,14},{12... | collective-permute-start | bytes 786440 | tf_op jit(solution)/shard_map/ppermute | solution.py:25
  75.3 12.5 %collective-permute-start.25 = (bf16[1024,128]{1,0:T(8,128)(2,1)S(1)}, bf16[1024,128]{1,0:T(8,128)(2,1)S(1)}, u32[]{:S(2)}, u32[]{:S(2)}) collective-permute-start(bf16[1024,128]{1,0:T(8,128)(2,1)S(1)} %get-tuple-element.39.rest_3_), channel_id=1, source_target_pairs={{0,2},{2,0},{4,6},{6,4},{1,3},{3,1},{5,7},{7,5},{8,10},{10,8},{12,... | collective-permute-start | bytes 786440 | tf_op jit(solution)/shard_map/ppermute | solution.py:25
  77.3 6.8 %collective-permute-start.23 = (f32[16,128]{1,0:T(8,128)S(1)}, f32[16,128]{1,0:T(8,128)S(1)}, u32[]{:S(2)}, u32[]{:S(2)}) collective-permute-start(f32[16,128]{1,0:T(8,128)S(1)} %add.9), channel_id=1, source_target_pairs={{0,2},{2,0},{4,6},{6,4},{1,3},{3,1},{5,7},{7,5},{8,10},{10,8},{12,... | collective-permute-start | bytes 24584 | tf_op jit(solution)/shard_map/ppermute | solution.py:25
  (12 other events, 253.6 us)
